TPU v7x, 32 devices: a whole 2x2x4 slice. The times are simulated.
32 devices in a mesh: sp: 16 (over z, y, x), tp: 2 (over core).
Axes of the slice: x: 2, y: 2, z: 4, core: 2. Of those that a mesh axis runs over, the one named last changes fastest.
Arguments:
- block_source: bfloat16 [2048, 2048], P('sp'), may hold values from -28 to 28
- address_weights: bfloat16 [1024, 2048], P('tp'), may hold values from -0.125 to 0.125
- causal_filter_taps: float32 [4, 1024], P(None, 'tp'), may hold values from -3 to 3
- payload_vectors: bfloat16 [2048, 2048], P('sp', 'tp'), may hold values from -0.25 to 0.25
- probe_vectors: bfloat16 [2048, 1024], P('sp', 'tp'), may hold values from -0.5 to 0.5
- interval_preimage: float32 [2048, 32], P('sp', 'tp'), may hold values from -3.5 to 4
- channel_damping_exponent: float32 [32], P('tp'), may hold values from -14 to -3
- added_damping_jumps: float32 [2048, 32], P('sp', 'tp'), may hold values from -1 to 0
- sigmoid_argument: bfloat16 [2048, 2048], P('sp', 'tp'), may hold values from -6 to 6
- adjoint_of_result: bfloat16 [2048, 2048], P('sp', 'tp'), may hold values from -6 to 6
Outputs:
- key_weight_grad: float32 [1024, 2048], P('tp', 'sp')
- row_squares: float32 [1024], P('tp')
- input_grad: bfloat16 [2048, 2048], P('tp', 'sp')
- value_grad: bfloat16 [2048, 2048], P('sp', 'tp')
- query_grad: bfloat16 [2048, 1024], P('sp', 'tp')
- decay_grad: float32 [2048, 32], P('sp', 'tp')
- gate_grad: bfloat16 [2048, 2048], P('sp', 'tp')
All inputs are finite; a program needn't handle non-finite values.
Results may differ from a plain program's by a relative error of at most 0.015.
Values may be sent and summed in bfloat16 or wider, within the bound.
A program may use at most 64 MiB of HBM per device.

v0:
```python
import jax
import jax.numpy as jnp
from jax import lax
from jax.sharding import PartitionSpec as P

STATE = 128
BLOCK = 128


HIGHEST = lax.Precision.HIGHEST


def from_partner(block, axis, bit):
    count = lax.axis_size(axis)
    route = []
    for low in range(count):
        high = low | 1 << bit
        if high != low and high < count:
            route += [(low, high), (high, low)]
    return lax.ppermute(block, axis, route)


def from_behind(block, axis, distance):
    devices = range(lax.axis_size(axis))
    route = [(i - distance, i) for i in devices if i - distance in devices]
    return lax.ppermute(block, axis, route)


def silu_slope(pre_act):
    sigma = jax.nn.sigmoid(pre_act)
    return sigma * (1.0 + pre_act * (1.0 - sigma))


def causal_conv(padded, causal_filter_taps, tokens):
    result = causal_filter_taps[0][None] * padded[0:tokens]
    for offset in range(1, causal_filter_taps.shape[0]):
        result = result + causal_filter_taps[offset][None] * padded[offset : offset + tokens]
    return result


def conv_transpose(extended, causal_filter_taps, tokens):
    tap_count = causal_filter_taps.shape[0]
    result = causal_filter_taps[0][None] * extended[tap_count - 1 : tap_count - 1 + tokens]
    for offset in range(1, tap_count):
        first_row = tap_count - 1 - offset
        result = (
            result + causal_filter_taps[offset][None] * extended[first_row : first_row + tokens]
        )
    return result


def block_step(carry_state, inputs):
    payload_vectors, damping_exponent, key_block, probe_vectors, step_block, scores = inputs
    block_len = payload_vectors.shape[0]
    scaled = payload_vectors * step_block[..., None]
    cumulative = jnp.cumsum(damping_exponent, axis=0)
    causal = jnp.tril(jnp.ones((block_len, block_len), dtype=bool))
    gaps = cumulative[:, None] - cumulative[None, :]
    decay_mat = jnp.exp(jnp.where(causal[:, :, None, None], gaps, -jnp.inf))
    within = jnp.einsum("gij,ijgr,jgrp->igrp", scores, decay_mat, scaled, precision=HIGHEST)
    carried = (
        jnp.einsum("ign,grpn->igrp", probe_vectors, carry_state, precision=HIGHEST)
        * jnp.exp(cumulative)[..., None]
    )
    end_decay = cumulative[-1]
    weights = jnp.exp(end_decay[None] - cumulative)
    new_state = carry_state * jnp.exp(end_decay)[..., None, None] + jnp.einsum(
        "jgn,jgr,jgrp->grpn", key_block, weights, scaled, precision=HIGHEST
    )
    return (new_state, within + carried)


def linear_scan_update(
    payload_vectors,
    interval_preimage,
    pooled_addresses,
    pooled_probes,
    blocked_scores,
    starting_memory,
    channel_damping_exponent,
    added_damping_jumps,
):
    tokens = pooled_addresses.shape[0]
    groups = pooled_addresses.shape[1]
    head_count = interval_preimage.shape[1]
    group_heads = head_count // groups
    block_count = tokens // BLOCK
    interval_widths = jax.nn.softplus(interval_preimage)
    damping_exponent = (
        added_damping_jumps - jnp.exp(channel_damping_exponent)[None] * interval_widths
    )

    def to_blocks(array):
        return array.reshape((block_count, BLOCK) + array.shape[1:])

    final_state, outputs = lax.scan(
        block_step,
        starting_memory,
        (
            to_blocks(payload_vectors.reshape(tokens, groups, group_heads, -1)),
            to_blocks(damping_exponent.reshape(tokens, groups, group_heads)),
            to_blocks(pooled_addresses),
            to_blocks(pooled_probes),
            to_blocks(interval_widths.reshape(tokens, groups, group_heads)),
            blocked_scores,
        ),
    )
    return (outputs.reshape(tokens, -1), final_state)


def join_carry(earlier, later):
    return (earlier[0] + later[0], earlier[1] * jnp.exp(later[0])[..., None, None] + later[1])


def pair_chains(span_decay, fwd_span, bwd_span):
    my_index = lax.axis_index("sp")
    levels = lax.axis_size("sp").bit_length() - 1
    pre_decay = jnp.zeros_like(span_decay)
    pre_state = jnp.zeros_like(fwd_span)
    suf_decay = jnp.zeros_like(span_decay)
    suf_grad = jnp.zeros_like(bwd_span)
    for bit_level in range(levels):
        peer_decay, peer_fwd, peer_bwd = from_partner(
            (span_decay, fwd_span, bwd_span), "sp", bit_level
        )
        is_upper = my_index // 2**bit_level % 2 == 1
        low_prefix = join_carry((peer_decay, peer_fwd), (pre_decay, pre_state))
        high_suffix = join_carry((peer_decay, peer_bwd), (suf_decay, suf_grad))
        fwd_after_low = join_carry((peer_decay, peer_fwd), (span_decay, fwd_span))[1]
        fwd_after_high = join_carry((span_decay, fwd_span), (peer_decay, peer_fwd))[1]
        bwd_after_low = join_carry((span_decay, bwd_span), (peer_decay, peer_bwd))[1]
        bwd_after_high = join_carry((peer_decay, peer_bwd), (span_decay, bwd_span))[1]
        pre_decay = jnp.where(is_upper, low_prefix[0], pre_decay)
        pre_state = jnp.where(is_upper, low_prefix[1], pre_state)
        suf_decay = jnp.where(is_upper, suf_decay, high_suffix[0])
        suf_grad = jnp.where(is_upper, suf_grad, high_suffix[1])
        fwd_span = jnp.where(is_upper, fwd_after_low, fwd_after_high)
        bwd_span = jnp.where(is_upper, bwd_after_low, bwd_after_high)
        span_decay = span_decay + peer_decay
    return (pre_state, suf_grad)


def per_device(
    block_source,
    address_weights,
    causal_filter_taps,
    payload_vectors,
    probe_vectors,
    interval_preimage,
    channel_damping_exponent,
    added_damping_jumps,
    sigmoid_argument,
    adjoint_of_result,
):
    tokens, feature_count = block_source.shape
    channels = address_weights.shape[0]
    groups = channels // STATE
    head_count = interval_preimage.shape[1]
    group_heads = head_count // groups
    block_count = tokens // BLOCK
    rim_rows = causal_filter_taps.shape[0] - 1
    projected = lax.dot_general(
        block_source, address_weights, (((1,), (1,)), ((), ())), preferred_element_type=jnp.float32
    ).astype(jnp.bfloat16)
    prev_rim = from_behind(projected[tokens - rim_rows :], "sp", 1)
    padded = jnp.concatenate([prev_rim, projected], axis=0).astype(jnp.float32)
    convolved = causal_conv(padded, causal_filter_taps, tokens)
    key_narrow = jax.nn.silu(convolved).astype(jnp.bfloat16).reshape(tokens, groups, STATE)
    pooled_addresses = key_narrow.astype(jnp.float32)
    query_narrow = probe_vectors.reshape(tokens, groups, STATE)
    pooled_probes = query_narrow.astype(jnp.float32)
    blocked_scores = jnp.einsum(
        "bign,bjgn->bgij",
        query_narrow.reshape(block_count, BLOCK, groups, STATE),
        key_narrow.reshape(block_count, BLOCK, groups, STATE),
        preferred_element_type=jnp.float32,
    )
    value_wide = payload_vectors.astype(jnp.float32)
    interval_widths = jax.nn.softplus(interval_preimage)
    damping_exponent = (
        added_damping_jumps - jnp.exp(channel_damping_exponent)[None] * interval_widths
    )
    running = jnp.cumsum(damping_exponent, axis=0)
    span_total = running[-1]
    scaled = (
        value_wide.reshape(tokens, groups, group_heads, -1)
        * interval_widths.reshape(tokens, groups, group_heads)[..., None]
    )
    local_state = jnp.einsum(
        "tgn,tgr,tgrp->grpn",
        pooled_addresses,
        jnp.exp(span_total[None] - running).reshape(tokens, groups, group_heads),
        scaled,
        precision=HIGHEST,
    )
    gate_wide = sigmoid_argument.astype(jnp.float32)
    grad_wide = adjoint_of_result.astype(jnp.float32)
    mixed_grad = grad_wide * jax.nn.silu(gate_wide)
    local_grad = jnp.einsum(
        "tgn,tgr,tgrp->grpn",
        pooled_probes,
        jnp.exp(running).reshape(tokens, groups, group_heads),
        mixed_grad.reshape(tokens, groups, group_heads, -1),
        precision=HIGHEST,
    )
    span_decay = span_total.reshape(groups, group_heads)
    incoming_state, grad_out = pair_chains(span_decay, local_state, local_grad)

    def mixer(
        payload_factor, interval_argument_factor, address_factor, probe_factor, score_operand
    ):
        return linear_scan_update(
            payload_factor,
            interval_argument_factor,
            address_factor,
            probe_factor,
            score_operand,
            incoming_state,
            channel_damping_exponent,
            added_damping_jumps,
        )

    mixer_pair, pullback = jax.vjp(
        mixer, value_wide, interval_preimage, pooled_addresses, pooled_probes, blocked_scores
    )
    mixer_out = mixer_pair[0]
    value_grad, decay_grad, key_state_grad, query_state_grad, score_grad = pullback(
        (mixed_grad, grad_out)
    )
    key_grad = key_state_grad + jnp.einsum(
        "bgij,bign->bjgn",
        score_grad,
        pooled_probes.reshape(block_count, BLOCK, groups, STATE),
        precision=HIGHEST,
    ).reshape(tokens, groups, STATE)
    query_grad = query_state_grad + jnp.einsum(
        "bgij,bjgn->bign",
        score_grad,
        pooled_addresses.reshape(block_count, BLOCK, groups, STATE),
        precision=HIGHEST,
    ).reshape(tokens, groups, STATE)
    gate_grad = (grad_wide * mixer_out * silu_slope(gate_wide)).astype(jnp.bfloat16)
    conv_grad = key_grad.reshape(tokens, channels) * silu_slope(convolved)
    next_rim = from_behind(conv_grad[:rim_rows], "sp", -1)
    extended = jnp.concatenate([conv_grad, next_rim], axis=0)
    projected_grad = conv_transpose(extended, causal_filter_taps, tokens).astype(jnp.bfloat16)
    input_grad = lax.psum_scatter(
        lax.dot_general(
            address_weights,
            projected_grad,
            (((0,), (1,)), ((), ())),
            preferred_element_type=jnp.float32,
        ).astype(jnp.bfloat16),
        "tp",
        scatter_dimension=0,
        tiled=True,
    )
    summed = lax.psum_scatter(
        lax.dot_general(
            block_source,
            projected_grad,
            (((0,), (0,)), ((), ())),
            preferred_element_type=jnp.float32,
        ),
        "sp",
        scatter_dimension=0,
        tiled=True,
    )
    key_weight_grad = summed.T
    row_squares = lax.psum(jnp.sum(summed * summed, axis=0), "sp")
    return (
        key_weight_grad,
        row_squares,
        input_grad,
        value_grad.astype(jnp.bfloat16),
        query_grad.reshape(tokens, channels).astype(jnp.bfloat16),
        decay_grad,
        gate_grad,
    )


def solution(mesh):
    in_specs = (
        P("sp", None),
        P("tp", None),
        P(None, "tp"),
        P("sp", "tp"),
        P("sp", "tp"),
        P("sp", "tp"),
        P("tp"),
        P("sp", "tp"),
        P("sp", "tp"),
        P("sp", "tp"),
    )
    out_specs = (
        P("tp", "sp"),
        P("tp"),
        P("tp", "sp"),
        P("sp", "tp"),
        P("sp", "tp"),
        P("sp", "tp"),
        P("sp", "tp"),
    )
    return jax.shard_map(
        per_device, mesh=mesh, in_specs=in_specs, out_specs=out_specs, check_vma=False
    )
```

profile of v0, /device:TPU:0, one launch (start us, length us, event | category | flops | bytes accessed | tf_op | source)
XLA Modules:
  0.0 319.1 jit_solution(17930630459186617223)
XLA Ops:
  10.6 3.0 collective-permute-start.1
  13.6 1.9 convolution_convert_fusion.1
  16.1 2.5 collective-permute-start.7
  21.0 2.4 collective-permute-start
  26.7 1.6 multiply_convert_fusion.1
  30.2 1.5 collective-permute-start.3
  31.8 2.1 collective-permute-done.3
  34.4 1.6 collective-permute-start.5
  36.0 2.0 collective-permute-done.5
  39.3 7.0 %collective-permute-done.9 = f32[4,4,64,128]{3,2,1,0:T(8,128)} collective-permute-done((f32[4,4,64,128]{3,2,1,0:T(8,128)}, f32[4,4,64,128]{3,2,1,0:T(8,128)}, u32[]{:S(2)}, u32[]{:S(2)}) %collective-permute-start.9) | collective-permute-done | bytes 524320 | tf_op jit(solution)/shard_map/ppermute | solution.py:20
  46.3 2.7 add_select_fusion.11
  52.0 12.1 %collective-permute-done.10 = f32[4,4,64,128]{3,2,1,0:T(8,128)} collective-permute-done((f32[4,4,64,128]{3,2,1,0:T(8,128)}, f32[4,4,64,128]{3,2,1,0:T(8,128)}, u32[]{:S(2)}, u32[]{:S(2)}) %collective-permute-start.10) | collective-permute-done | bytes 524320 | tf_op jit(solution)/shard_map/ppermute | solution.py:20
  64.2 9.0 %collective-permute-done.2 = f32[4,4,64,128]{3,2,1,0:T(8,128)} collective-permute-done((f32[4,4,64,128]{3,2,1,0:T(8,128)}, f32[4,4,64,128]{3,2,1,0:T(8,128)}, u32[]{:S(2)}, u32[]{:S(2)}) %collective-permute-start.2) | collective-permute-done | bytes 524320 | tf_op jit(solution)/shard_map/ppermute | solution.py:20
  73.1 1.8 add_select_fusion.10
  74.9 1.6 collective-permute-start.11
  77.9 11.9 %collective-permute-done.11 = f32[4,4,64,128]{3,2,1,0:T(8,128)S(1)} collective-permute-done((f32[4,4,64,128]{3,2,1,0:T(8,128)S(1)}, f32[4,4,64,128]{3,2,1,0:T(8,128)S(1)}, u32[]{:S(2)}, u32[]{:S(2)}) %collective-permute-start.11) | collective-permute-done | bytes 524320 | tf_op jit(solution)/shard_map/ppermute | solution.py:20
  89.8 8.1 %collective-permute-done.4 = f32[4,4,64,128]{3,2,1,0:T(8,128)S(1)} collective-permute-done((f32[4,4,64,128]{3,2,1,0:T(8,128)S(1)}, f32[4,4,64,128]{3,2,1,0:T(8,128)S(1)}, u32[]{:S(2)}, u32[]{:S(2)}) %collective-permute-start.4) | collective-permute-done | bytes 524320 | tf_op jit(solution)/shard_map/ppermute | solution.py:20
  99.2 2.6 collective-permute-start.12
  102.8 1.7 copy.102
  104.5 3.6 %fusion.3 = (f32[4,128,128]{2,1,0:T(8,128)S(1)}, f32[4,4,128,128]{3,2,1,0:T(8,128)}) fusion(f32[128,4,4]{0,2,1:T(4,128)S(1)} %copy.105, pred[128,128]{1,0:T(8,128)(4,1)} %iota_compare_fusion, f32[4,4,128,64]{2,3,1,0:T(8,128)S(1)} %bitcast.126, f32[128,4,4,64]{0,3,2,1:T(8,128)S(1)} %bitcast.130, f32[128,4,4]{0,2,1:T(4,128)S(1)} %bitcast.147), kind=kOutput, calls=%fused_computation.12 | convolution fusion | flops 202440704 | bytes 2392064 | tf_op jit(solution)/shard_map/transpose(jvp())/while/body/eval_jaxpr/gij,ijgr,jgrp->igrp/dot_general | solution.py:60
  109.8 1.8 copy.109
  111.6 23.1 %collective-permute-done.12 = f32[4,4,64,128]{3,2,1,0:T(8,128)} collective-permute-done((f32[4,4,64,128]{3,2,1,0:T(8,128)}, f32[4,4,64,128]{3,2,1,0:T(8,128)}, u32[]{:S(2)}, u32[]{:S(2)}) %collective-permute-start.12) | collective-permute-done | bytes 524320 | tf_op jit(solution)/shard_map/ppermute | solution.py:20
  134.8 10.2 %collective-permute-done.6 = f32[4,4,64,128]{3,2,1,0:T(8,128)} collective-permute-done((f32[4,4,64,128]{3,2,1,0:T(8,128)}, f32[4,4,64,128]{3,2,1,0:T(8,128)}, u32[]{:S(2)}, u32[]{:S(2)}) %collective-permute-start.6) | collective-permute-done | bytes 524320 | tf_op jit(solution)/shard_map/ppermute | solution.py:20
  144.9 4.0 %multiply_reduce_fusion.2 = (f32[4,4]{1,0:T(4,128)}, f32[4,4,64,128]{3,2,1,0:T(8,128)}, f32[4,4,64,128]{3,2,1,0:T(8,128)S(1)}) fusion(f32[4,4,64,128]{3,2,1,0:T(8,128)} %collective-permute-done.9, pred[]{:T(512)S(6)} %eq.28, f32[4,4,64,128]{3,2,1,0:T(8,128)} %collective-permute-done.10, f32[4,4]{1,0:T(4,128)} %get-tuple-element.210, pred[]{:T(512)S(6)} %eq.27, ...), kind=kLoop, calls=%fused_computation.42 | loop fusion | flops 2883568 | bytes 5243332 | tf_op jit(solution)/shard_map/transpose(jvp())/while/body/eval_jaxpr/reduce_sum | solution.py:67
  149.7 1.8 fusion.31
  151.5 1.8 copy.108
  155.8 4.2 %collective-permute-done.8 = f32[3,512]{1,0:T(4,128)S(1)} collective-permute-done((f32[3,512]{1,0:T(4,128)S(1)}, f32[3,512]{1,0:T(4,128)S(1)}, u32[]{:S(2)}, u32[]{:S(2)}) %collective-permute-start.8) | collective-permute-done | bytes 6176 | tf_op jit(solution)/shard_map/ppermute | solution.py:26
  163.1 3.8 %convolution_bitcast_fusion = f32[2048,512]{0,1:T(8,128)} fusion(bf16[128,512]{1,0:T(8,128)(2,1)} %copy-done.10, bf16[128,2048]{1,0:T(8,128)(2,1)} %param.10), kind=kOutput, calls=%fused_computation | convolution fusion | flops 268435456 | bytes 4849664 | tf_op jit(solution)/shard_map/dot_general | solution.py:259
  170.3 1.9 convolution_bitcast_fusion.5
  172.3 1.8 copy.113
  174.0 2.6 fusion.10
  176.6 1.6 copy.121
  178.2 1.5 copy.122
  179.7 2.1 fusion.86
  181.9 1.8 copy.118
  185.1 3.6 %multiply_reduce_fusion = (f32[128,4,4]{0,2,1:T(4,128)}, f32[128,4,4]{0,2,1:T(4,128)}, bf16[128,4,4,64]{0,3,2,1:T(8,128)(2,1)}) fusion(f32[128,4,4,64]{0,3,2,1:T(8,128)S(1)} %convolution_bitcast_fusion.4, f32[128,4,4]{0,2,1:T(4,128)S(1)} %bitcast.149, f32[128,1024]{0,1:T(8,128)S(1)} %copy.103, f32[4,4,128,64]{2,3,1,0:T(8,128)S(1)} %bitcast.127, ...), kind=kOutput, calls=%fused_computation.40 | convolution fusion | flops 203288576 | bytes 2154496 | tf_op jit(solution)/shard_map/transpose(jvp())/while/body/eval_jaxpr/gij,ijgr,jgrp->igrp/dot_general | solution.py:60
  188.7 1.6 copy.148
  190.3 2.8 multiply_reduce_fusion.1
  193.1 1.6 copy.120
  196.4 2.2 add_add_fusion
  199.8 4.2 %fusion.1 = f32[128,4,4,64]{0,3,2,1:T(8,128)} fusion(f32[128,4,4,64]{0,3,2,1:T(8,128)} %get-tuple-element.218, f32[128,128,4]{1,0,2:T(8,128)} %copy.113, f32[128,4,4]{0,2,1:T(4,128)S(1)} %copy.105, pred[128,128]{1,0:T(8,128)(4,1)S(1)} %copy-done.17, f32[128,4,4,64]{0,3,2,1:T(8,128)S(1)} %bitcast.132, f32[128,4,4]{0,2,1:T(4,128)S(1)} %copy.114, ...), kind=kOutput, calls=%fused_computation.4 | convolution fusion | flops 202506240 | bytes 1875968 | tf_op jit(solution)/shard_map/jvp()/while/body/eval_jaxpr/gij,ijgr,jgrp->igrp/dot_general | solution.py:60
  204.0 2.1 copy.129
  209.5 1.8 copy.131
  211.3 1.6 add_convert_fusion
  213.0 2.1 fusion.12
  215.1 1.8 copy.130
  216.9 53.7 %reduce-scatter.3.cloned.1.call-done = f32[128,512]{0,1:T(8,128)} async-done(((f32[2048,512]{0,1:T(8,128)}), f32[128,512]{0,1:T(8,128)}) %reduce-scatter.3.cloned.1.call-update) | async-done | bytes 262160 | tf_op jit(solution)/shard_map/reduce_scatter | solution.py:258
  271.7 40.5 %psum.7 = f32[512]{0:T(512)} all-reduce(f32[512]{0:T(512)S(1)} %multiply_reduce_fusion.4), channel_id=1, replica_groups=mesh['sp'=16,'tp'=2] {'sp'}, use_global_device_ids=true, to_apply=%region_4.5 | all-reduce | flops 512 | bytes 4096 | tf_op jit(solution)/shard_map/psum | solution.py:270
  (119 shorter events, 40.4 us)
Async XLA Ops:
  7.2 6.4 %copy-start = (bf16[512,2048]{1,0:T(8,128)(2,1)S(1)}, bf16[512,2048]{1,0:T(8,128)(2,1)}, u32[]{:S(2)}) copy-start(bf16[512,2048]{1,0:T(8,128)(2,1)} %param.11) | copy-start | bytes 6291460
  7.2 12.2 %copy-start.13 = (bf16[128,1024]{1,0:T(8,128)(2,1)S(1)}, bf16[128,1024]{1,0:T(8,128)(2,1)}, u32[]{:S(2)}) copy-start(bf16[128,1024]{1,0:T(8,128)(2,1)} %param.18) | copy-start | bytes 786436
  7.2 12.2 %copy-start.12 = (bf16[128,1024]{1,0:T(8,128)(2,1)S(1)}, bf16[128,1024]{1,0:T(8,128)(2,1)}, u32[]{:S(2)}) copy-start(bf16[128,1024]{1,0:T(8,128)(2,1)} %param.19) | copy-start | bytes 786436
  7.2 207.9 %reduce-scatter.5.cloned.1.call-start = ((), (), s32[]{:S(2)}) async-start(), calls=%async_computation.3 | async-start | bytes 786432 | tf_op jit(solution)/shard_map/reduce_scatter | solution.py:247
  8.2 10.4 %copy-start.15 = (f32[128,16]{1,0:T(8,128)}, f32[128,16]{1,0:T(8,128)S(1)}, u32[]{:S(2)}) copy-start(f32[128,16]{1,0:T(8,128)S(1)} %copy.91) | copy-start | bytes 24580
  8.9 1.7 copy-start.24
  10.6 9.2 %copy-start.6 = (bf16[128,512]{1,0:T(8,128)(2,1)S(1)}, bf16[128,512]{1,0:T(8,128)(2,1)}, u32[]{:S(2)}) copy-start(bf16[128,512]{1,0:T(8,128)(2,1)} %param.14) | copy-start | bytes 393220
  10.6 18.9 %collective-permute-start.1 = (f32[4,4]{1,0:T(4,128)}, f32[4,4]{1,0:T(4,128)}, u32[]{:S(2)}, u32[]{:S(2)}) collective-permute-start(f32[4,4]{1,0:T(4,128)} %reshape_squeeze.3), channel_id=1, source_target_pairs={{0,2},{2,0},{4,6},{6,4},{8,10},{10,8},{12,14},{14,12},{16,18},{18,... | collective-permute-start | bytes 200 | tf_op jit(solution)/shard_map/ppermute | solution.py:20
  16.1 10.0 %collective-permute-start.7 = (bf16[3,512]{1,0:T(4,128)(2,1)}, bf16[3,512]{1,0:T(4,128)(2,1)}, u32[]{:S(2)}, u32[]{:S(2)}) collective-permute-start(bf16[3,512]{1,0:T(4,128)(2,1)} %slice.67), channel_id=1, source_target_pairs={{0,2},{2,4},{4,6},{6,8},{8,10},{10,12},{12,14},{14,16},{16,18},{18... | collective-permute-start | bytes 9224 | tf_op jit(solution)/shard_map/ppermute | solution.py:26
  19.8 5.0 %copy-start.8 = (bf16[128,4,128]{2,1,0:T(4,128)(2,1)}, bf16[128,4,128]{2,1,0:T(4,128)(2,1)S(1)}, u32[]{:S(2)}) copy-start(bf16[128,4,128]{2,1,0:T(4,128)(2,1)S(1)} %reshape.188) | copy-start | bytes 393220
  21.0 18.3 %collective-permute-start = (f32[4,4,64,128]{3,2,1,0:T(8,128)}, f32[4,4,64,128]{3,2,1,0:T(8,128)}, u32[]{:S(2)}, u32[]{:S(2)}) collective-permute-start(f32[4,4,64,128]{3,2,1,0:T(8,128)} %fusion.33), channel_id=1, source_target_pairs={{0,2},{2,0},{4,6},{6,4},{8,10},{10,8},{12,14},{14,12},{16,18},{18,... | collective-permute-start | bytes 1572872 | tf_op jit(solution)/shard_map/ppermute | solution.py:20
  29.5 16.8 %collective-permute-start.9 = (f32[4,4,64,128]{3,2,1,0:T(8,128)}, f32[4,4,64,128]{3,2,1,0:T(8,128)}, u32[]{:S(2)}, u32[]{:S(2)}) collective-permute-start(f32[4,4,64,128]{3,2,1,0:T(8,128)} %fusion.20), channel_id=1, source_target_pairs={{0,2},{2,0},{4,6},{6,4},{8,10},{10,8},{12,14},{14,12},{16,18},{18,... | collective-permute-start | bytes 1572872 | tf_op jit(solution)/shard_map/ppermute | solution.py:20
  30.2 3.6 %collective-permute-start.3 = (f32[4,4]{1,0:T(4,128)S(1)}, f32[4,4]{1,0:T(4,128)S(1)}, u32[]{:S(2)}, u32[]{:S(2)}) collective-permute-start(f32[4,4]{1,0:T(4,128)S(1)} %get-tuple-element.161), channel_id=1, source_target_pairs={{0,4},{4,0},{2,6},{6,2},{8,12},{12,8},{10,14},{14,10},{16,20},{20,... | collective-permute-start | bytes 200 | tf_op jit(solution)/shard_map/ppermute | solution.py:20
  34.4 3.6 %collective-permute-start.5 = (f32[4,4]{1,0:T(4,128)S(1)}, f32[4,4]{1,0:T(4,128)S(1)}, u32[]{:S(2)}, u32[]{:S(2)}) collective-permute-start(f32[4,4]{1,0:T(4,128)S(1)} %get-tuple-element.159), channel_id=1, source_target_pairs={{0,8},{8,0},{2,10},{10,2},{4,12},{12,4},{6,14},{14,6},{16,24},{24,... | collective-permute-start | bytes 200 | tf_op jit(solution)/shard_map/ppermute | solution.py:20
  49.1 15.1 %collective-permute-start.10 = (f32[4,4,64,128]{3,2,1,0:T(8,128)}, f32[4,4,64,128]{3,2,1,0:T(8,128)}, u32[]{:S(2)}, u32[]{:S(2)}) collective-permute-start(f32[4,4,64,128]{3,2,1,0:T(8,128)} %get-tuple-element.208), channel_id=1, source_target_pairs={{0,4},{4,0},{2,6},{6,2},{8,12},{12,8},{10,14},{14,10},{16,20},{20,... | collective-permute-start | bytes 1572872 | tf_op jit(solution)/shard_map/ppermute | solution.py:20
  50.6 22.6 %collective-permute-start.2 = (f32[4,4,64,128]{3,2,1,0:T(8,128)}, f32[4,4,64,128]{3,2,1,0:T(8,128)}, u32[]{:S(2)}, u32[]{:S(2)}) collective-permute-start(f32[4,4,64,128]{3,2,1,0:T(8,128)} %get-tuple-element.207), channel_id=1, source_target_pairs={{0,4},{4,0},{2,6},{6,2},{8,12},{12,8},{10,14},{14,10},{16,20},{20,... | collective-permute-start | bytes 1572872 | tf_op jit(solution)/shard_map/ppermute | solution.py:20
  52.0 25.0 %copy-start.14 = (f32[128,4,4]{2,1,0:T(4,128)S(1)}, f32[128,4,4]{2,1,0:T(4,128)}, u32[]{:S(2)}) copy-start(f32[128,4,4]{2,1,0:T(4,128)} %copy.101) | copy-start | bytes 24580
  73.1 24.8 %copy-start.22 = (f32[4,4]{1,0:T(4,128)S(1)}, f32[4,4]{1,0:T(4,128)}, u32[]{:S(2)}) copy-start(f32[4,4]{1,0:T(4,128)} %get-tuple-element.213) | copy-start | bytes 196
  73.1 24.8 %copy-start.23 = (f32[4,4]{1,0:T(4,128)S(1)}, f32[4,4]{1,0:T(4,128)}, u32[]{:S(2)}) copy-start(f32[4,4]{1,0:T(4,128)} %get-tuple-element.158) | copy-start | bytes 196
  74.9 14.9 %collective-permute-start.11 = (f32[4,4,64,128]{3,2,1,0:T(8,128)S(1)}, f32[4,4,64,128]{3,2,1,0:T(8,128)S(1)}, u32[]{:S(2)}, u32[]{:S(2)}) collective-permute-start(f32[4,4,64,128]{3,2,1,0:T(8,128)S(1)} %get-tuple-element.206), channel_id=1, source_target_pairs={{0,8},{8,0},{2,10},{10,2},{4,12},{12,4},{6,14},{14,6},{16,24},{24,... | collective-permute-start | bytes 1572872 | tf_op jit(solution)/shard_map/ppermute | solution.py:20
  76.6 21.4 %collective-permute-start.4 = (f32[4,4,64,128]{3,2,1,0:T(8,128)S(1)}, f32[4,4,64,128]{3,2,1,0:T(8,128)S(1)}, u32[]{:S(2)}, u32[]{:S(2)}) collective-permute-start(f32[4,4,64,128]{3,2,1,0:T(8,128)S(1)} %get-tuple-element.205), channel_id=1, source_target_pairs={{0,8},{8,0},{2,10},{10,2},{4,12},{12,4},{6,14},{14,6},{16,24},{24,... | collective-permute-start | bytes 1572872 | tf_op jit(solution)/shard_map/ppermute | solution.py:20
  77.2 25.6 %copy-start.19 = (f32[4,4]{1,0:T(4,128)}, f32[4,4]{1,0:T(4,128)S(1)}, u32[]{:S(2)}) copy-start(f32[4,4]{1,0:T(4,128)S(1)} %slice_bitcast_fusion) | copy-start | bytes 196
  89.8 8.1 %copy-start.4 = (f32[4,4,64,128]{3,2,1,0:T(8,128)}, f32[4,4,64,128]{3,2,1,0:T(8,128)S(1)}, u32[]{:S(2)}) copy-start(f32[4,4,64,128]{3,2,1,0:T(8,128)S(1)} %collective-permute-done.11) | copy-start | bytes 1572868
  97.9 1.3 copy-start.5
  99.2 35.6 %collective-permute-start.12 = (f32[4,4,64,128]{3,2,1,0:T(8,128)}, f32[4,4,64,128]{3,2,1,0:T(8,128)}, u32[]{:S(2)}, u32[]{:S(2)}) collective-permute-start(f32[4,4,64,128]{3,2,1,0:T(8,128)} %get-tuple-element.204), channel_id=1, source_target_pairs={{0,16},{16,0},{2,18},{18,2},{4,20},{20,4},{6,22},{22,6},{8,24},{24... | collective-permute-start | bytes 1572872 | tf_op jit(solution)/shard_map/ppermute | solution.py:20
  101.8 43.2 %collective-permute-start.6 = (f32[4,4,64,128]{3,2,1,0:T(8,128)}, f32[4,4,64,128]{3,2,1,0:T(8,128)}, u32[]{:S(2)}, u32[]{:S(2)}) collective-permute-start(f32[4,4,64,128]{3,2,1,0:T(8,128)} %get-tuple-element.203), channel_id=1, source_target_pairs={{0,16},{16,0},{2,18},{18,2},{4,20},{20,4},{6,22},{22,6},{8,24},{24... | collective-permute-start | bytes 1572872 | tf_op jit(solution)/shard_map/ppermute | solution.py:20
  104.5 4.3 %copy-start.7 = (bf16[128,512]{1,0:T(8,128)(2,1)S(1)}, bf16[128,512]{1,0:T(8,128)(2,1)}, u32[]{:S(2)}) copy-start(bf16[128,512]{1,0:T(8,128)(2,1)} %param.14) | copy-start | bytes 393220
  108.1 0.7 copy-start.3
  144.9 4.8 %copy-start.20 = (f32[128,4,4]{0,2,1:T(4,128)S(1)}, f32[128,4,4]{0,2,1:T(4,128)}, u32[]{:S(2)}) copy-start(f32[128,4,4]{0,2,1:T(4,128)} %copy.102) | copy-start | bytes 24580
  148.9 0.8 copy-start.2
  154.5 5.5 %collective-permute-start.8 = (f32[3,512]{1,0:T(4,128)S(1)}, f32[3,512]{1,0:T(4,128)S(1)}, u32[]{:S(2)}, u32[]{:S(2)}) collective-permute-start(f32[3,512]{1,0:T(4,128)S(1)} %slice.72), channel_id=1, source_target_pairs={{2,0},{4,2},{6,4},{8,6},{10,8},{12,10},{14,12},{16,14},{18,16},{20... | collective-permute-start | bytes 18440 | tf_op jit(solution)/shard_map/ppermute | solution.py:26
  160.9 0.7 copy-start.10
  162.8 107.8 %reduce-scatter.3.cloned.1.call-start = ((), (), s32[]{:S(2)}) async-start(), calls=%async_computation.2 | async-start | bytes 4456448 | tf_op jit(solution)/shard_map/reduce_scatter | solution.py:258
  185.1 5.2 %copy-start.9 = (bf16[128,4,128]{2,1,0:T(4,128)(2,1)S(1)}, bf16[128,4,128]{2,1,0:T(4,128)(2,1)}, u32[]{:S(2)}) copy-start(bf16[128,4,128]{2,1,0:T(4,128)(2,1)} %copy-done.8) | copy-start | bytes 393220
  193.1 6.7 %copy-start.17 = (pred[128,128]{1,0:T(8,128)(4,1)S(1)}, pred[128,128]{1,0:T(8,128)(4,1)}, u32[]{:S(2)}) copy-start(pred[128,128]{1,0:T(8,128)(4,1)} %iota_compare_fusion) | copy-start | bytes 49156
  198.7 7.4 %copy-start.11 = (f32[128,4,4]{2,1,0:T(4,128)S(1)}, f32[128,4,4]{2,1,0:T(4,128)}, u32[]{:S(2)}) copy-start(f32[128,4,4]{2,1,0:T(4,128)} %get-tuple-element.163) | copy-start | bytes 24580
  198.7 8.8 %copy-start.21 = (f32[128,4,4]{0,2,1:T(4,128)S(1)}, f32[128,4,4]{0,2,1:T(4,128)}, u32[]{:S(2)}) copy-start(f32[128,4,4]{0,2,1:T(4,128)} %get-tuple-element.152) | copy-start | bytes 24580
  198.7 8.9 %copy-start.16 = (f32[128,16]{1,0:T(8,128)S(1)}, f32[128,16]{1,0:T(8,128)}, u32[]{:S(2)}) copy-start(f32[128,16]{1,0:T(8,128)} %copy-done.15) | copy-start | bytes 24580
  198.7 8.9 %copy-start.18 = (pred[128,16]{1,0:T(8,128)(4,1)S(1)}, pred[128,16]{1,0:T(8,128)(4,1)}, u32[]{:S(2)}) copy-start(pred[128,16]{1,0:T(8,128)(4,1)} %copy.127) | copy-start | bytes 6148
  198.7 8.9 %copy-start.25 = (f32[16]{0:T(128)S(1)}, f32[16]{0:T(128)}, u32[]{:S(2)}) copy-start(f32[16]{0:T(128)} %copy-done.24) | copy-start | bytes 196
  204.0 4.3 %copy-start.1 = (f32[4,4,64,128]{3,2,1,0:T(8,128)S(1)}, f32[4,4,64,128]{3,2,1,0:T(8,128)}, u32[]{:S(2)}) copy-start(f32[4,4,64,128]{3,2,1,0:T(8,128)} %get-tuple-element.154) | copy-start | bytes 1572868
Sparse Core Ops, SparseCore 0:
  163.0 8.3 reduce-scatter.4
  174.2 96.3 reduce-scatter.2
where the time goes:
time: 321 us; the launch traced here: 319 us
  waiting for transfers between devices  144 us (45%)
  blocking collectives  40.5 us (13%)
  local copies, waits for them, and re-layouts  35 us (11%)
  other arithmetic  33.2 us (10%)
  matrix products  32.9 us (10%)
  starting transfers between devices  19.5 us (6%)
  between operations  14.4 us (4%)
    ppermute x11, waiting for transfers between devices, from_partner(): return lax.ppermute(block, axis, route)  85.5 us
    reduce_scatter x1, waiting for transfers between devices, per_device(): lax.psum_scatter(lax.dot_general(block_source, projected_grad, (((0,), (0...  53.7 us
    psum x1, blocking collectives, per_device(): row_squares = lax.psum(jnp.sum(summed * summed, axis=0), 'sp')  40.5 us
    ppermute x11, starting transfers between devices, from_partner(): return lax.ppermute(block, axis, route)  15.5 us
    dot_general x3, matrix products, block_step(): jnp.einsum('gij,ijgr,jgrp->igrp', scores, decay_mat, scaled, precision=HI...  11.5 us
    unnamed x58, local copies, waits for them, and re-layouts  8.25 us
  transfers between devices with their start and end apart: 15, of which 11 were waited for; matrix products, arithmetic and copies ran while one was open for 24% of the time, Pallas kernels for 0%

commit v1 on v0

v1 whole, which is shorter than its diff:
```python
import functools

import jax
import jax.numpy as jnp
from jax import lax
from jax.experimental import pallas as pl
from jax.experimental.pallas import tpu as pltpu
from jax.sharding import PartitionSpec as P

STATE = 128
F32 = jnp.float32
BF16 = jnp.bfloat16
HIGHEST = lax.Precision.HIGHEST
MESH = pl.DeviceIdType.MESH


def dot(lhs, rhs, left=1, right=0, precision=None):
    return lax.dot_general(
        lhs,
        rhs,
        (((left,), (right,)), ((), ())),
        preferred_element_type=F32,
        precision=precision,
    )


def silu_slope(pre_act):
    sigma = jax.nn.sigmoid(pre_act)
    return sigma * (1.0 + pre_act * (1.0 - sigma))


def kernel(
    cfg,
    x_ref,
    w_ref,
    taps_ref,
    val_ref,
    qry_ref,
    pre_ref,
    damp_ref,
    jump_ref,
    gate_ref,
    adj_ref,
    kwg_ref,
    rows_ref,
    ig_ref,
    vg_ref,
    qg_ref,
    dg_ref,
    gg_ref,
    xh,
    pext,
    slope,
    cta,
    u_s,
    dy_s,
    dte_s,
    ece_s,
    wee_s,
    y_s,
    du_s,
    dq_s,
    dk_s,
    s_af,
    s_ab,
    r_af,
    r_ab,
    s_bf,
    s_bb,
    r_bf,
    r_bb,
    acc_f,
    acc_b,
    wgt_f,
    wgt_b,
    s_cf,
    s_cb,
    r_cf,
    r_cb,
    ext,
    halo,
    gbuf,
    xbuf,
    rsum,
    s_r,
    r_r,
    s_i,
    r_i,
    sq,
    sem_halo,
    sem_ct,
    sem_a,
    sem_b,
    sem_c,
    sem_x,
    sem_d,
    sem_r,
    sem_i,
    sem_q,
):
    nsp, ntp, outer, inner = cfg
    i = lax.axis_index("sp")
    p = lax.axis_index("tp")
    a = i // inner
    b = i % inner
    tokens, feats = x_ref.shape
    chans = w_ref.shape[0]
    heads = pre_ref.shape[1]
    hdim = val_ref.shape[1] // heads
    groups = chans // STATE
    gcols = val_ref.shape[1] // groups
    qheads = heads // inner
    qrows = qheads * hdim
    span = feats // outer
    piece = feats // nsp
    fchunk = feats // ntp

    barrier = pltpu.get_barrier_semaphore()
    for o in range(1, nsp):
        pl.semaphore_signal(
            barrier, inc=1, device_id={"sp": (i + o) % nsp}, device_id_type=MESH
        )
    for o in range(1, ntp):
        pl.semaphore_signal(
            barrier, inc=1, device_id={"tp": (p + o) % ntp}, device_id_type=MESH
        )

    pending = []

    def send(src, dst, ssem, rsem, device, when=None):
        copy = pltpu.make_async_remote_copy(
            src_ref=src,
            dst_ref=dst,
            send_sem=ssem,
            recv_sem=rsem,
            device_id=device,
            device_id_type=MESH,
        )
        if when is None:
            copy.start()
        else:
            pl.when(when)(copy.start)
        pending.append((copy, when))

    def arrive(dst, rsem):
        pltpu.make_async_copy(dst, dst, rsem).wait()

    def at_plane(other):
        return {"sp": a * inner + other}

    def at_outer(other):
        return {"sp": other * inner + b}

    row = lax.broadcasted_iota(jnp.int32, (tokens, tokens), 0)
    col = lax.broadcasted_iota(jnp.int32, (tokens, tokens), 1)
    lower = (col <= row).astype(F32)
    upper = (row <= col).astype(F32)
    eh = lax.broadcasted_iota(jnp.int32, (heads, heads * hdim), 0)
    ec = lax.broadcasted_iota(jnp.int32, (heads, heads * hdim), 1)
    expand = (ec // hdim == eh).astype(F32)

    pre = pre_ref[...]
    rate = jnp.exp(damp_ref[...])
    step = jnp.maximum(pre, 0.0) + jnp.log1p(jnp.exp(-jnp.abs(pre)))
    decay = jump_ref[...] - rate * step
    cum = dot(lower, decay, precision=HIGHEST)
    cum_t = dot(decay, upper, 0, 0, precision=HIGHEST)
    total = dot(decay, jnp.ones((tokens, STATE), F32), 0, 0, precision=HIGHEST)
    for k in range(inner):
        cta[i, k] = total[k * qheads : (k + 1) * qheads]
    end = cum[tokens - 1 : tokens]

    pl.semaphore_wait(barrier, nsp - 1 + ntp - 1)

    send(
        x_ref.at[pl.ds(tokens - 16, 16)],
        xh,
        sem_halo.at[0],
        sem_halo.at[1],
        {"sp": (i + 1) % nsp},
        i < nsp - 1,
    )
    for o in range(1, nsp):
        peer = (i + o) % nsp
        send(cta.at[i], cta.at[i], sem_ct.at[0, o], sem_ct.at[1, i], {"sp": peer})

    ece = dot(jnp.exp(cum), expand, precision=HIGHEST)
    ece_s[...] = ece
    gate = gate_ref[...].astype(F32)
    dy = adj_ref[...].astype(F32) * (gate * jax.nn.sigmoid(gate))
    dy_s[...] = dy.astype(BF16)
    edy = (dy * ece).astype(BF16)
    for g in range(groups):
        cs = slice(g * gcols, (g + 1) * gcols)
        part = dot(edy[:, cs], qry_ref[:, g * STATE : (g + 1) * STATE], 0, 0)
        s_ab[pl.ds(g * gcols, gcols)] = part.astype(BF16)
    for o in range(1, inner):
        peer = (b + o) % inner
        send(
            s_ab.at[pl.ds(pl.multiple_of(peer * qrows, qrows), qrows)],
            r_ab.at[b],
            sem_a.at[0, 0, o],
            sem_a.at[0, 1, b],
            at_plane(peer),
        )
    r_ab[b] = s_ab[pl.ds(pl.multiple_of(b * qrows, qrows), qrows)]

    for o in range(1, outer):
        peer = (a + o) % outer
        send(
            x_ref.at[:, pl.ds(pl.multiple_of(peer * span, span), span)],
            xbuf.at[a],
            sem_x.at[0, o],
            sem_x.at[1, a],
            at_outer(peer),
        )
    xbuf[a] = x_ref[:, pl.ds(pl.multiple_of(a * span, span), span)]

    dte = dot(step, expand, precision=HIGHEST)
    dte_s[...] = dte
    wee = dot(jnp.exp(end - cum), expand, precision=HIGHEST)
    wee_s[...] = wee
    scaled = val_ref[...].astype(F32) * dte
    u_s[...] = scaled.astype(BF16)
    wu = (scaled * wee).astype(BF16)

    proj = dot(x_ref[...], w_ref[...], 1, 1)
    pext[pl.ds(16, tokens)] = proj.astype(BF16).astype(F32)

    @pl.when(i > 0)
    def _():
        arrive(xh, sem_halo.at[1])
        pext[pl.ds(0, 16)] = dot(xh[...], w_ref[...], 1, 1).astype(BF16).astype(F32)

    @pl.when(i == 0)
    def _():
        pext[pl.ds(0, 16)] = jnp.zeros((16, chans), F32)

    taps = taps_ref[...]
    ntap = taps_ref.shape[0]
    conv = taps[0:1] * pext[pl.ds(16 - (ntap - 1), tokens)]
    for k in range(1, ntap):
        conv = conv + taps[k : k + 1] * pext[pl.ds(16 - (ntap - 1) + k, tokens)]
    slope[...] = silu_slope(conv)
    keys = (conv * jax.nn.sigmoid(conv)).astype(BF16)

    for g in range(groups):
        cs = slice(g * gcols, (g + 1) * gcols)
        part = dot(wu[:, cs], keys[:, g * STATE : (g + 1) * STATE], 0, 0)
        s_af[pl.ds(g * gcols, gcols)] = part.astype(BF16)
    for o in range(1, inner):
        peer = (b + o) % inner
        send(
            s_af.at[pl.ds(pl.multiple_of(peer * qrows, qrows), qrows)],
            r_af.at[b],
            sem_a.at[1, 0, o],
            sem_a.at[1, 1, b],
            at_plane(peer),
        )
    r_af[b] = s_af[pl.ds(pl.multiple_of(b * qrows, qrows), qrows)]

    causal = col <= row

    def within(g):
        gs = slice(g * STATE, (g + 1) * STATE)
        q = qry_ref[:, gs]
        key = keys[:, gs]
        scores = dot(q, key, 1, 1)
        dscore = jnp.zeros((tokens, tokens), F32)
        for h in range(g * gcols // hdim, (g + 1) * gcols // hdim):
            hs = slice(h * hdim, (h + 1) * hdim)
            gap = cum[:, h : h + 1] - cum_t[h : h + 1, :]
            damp = jnp.exp(jnp.where(causal, gap, -jnp.inf))
            mixed = (scores * damp).astype(BF16)
            u = u_s[:, hs]
            d = dy_s[:, hs]
            dscore = dscore + dot(d, u, 1, 1) * damp
            y_s[:, hs] = dot(mixed, u)
            du_s[:, hs] = dot(mixed, d, 0, 0)
        ds = dscore.astype(BF16)
        dq_s[:, gs] = dot(ds, key)
        dk_s[:, gs] = dot(ds, q, 0, 0)

    cut1 = (groups + 1) // 2
    cut2 = cut1 + (groups - cut1 + 1) // 2
    for g in range(cut1):
        within(g)

    for o in range(1, nsp):
        src = (i + nsp - o) % nsp
        arrive(cta.at[src], sem_ct.at[1, src])

    def spread(rows):
        return jnp.concatenate(
            [jnp.broadcast_to(rows[h : h + 1], (hdim, STATE)) for h in range(qheads)], axis=0
        )

    for o in range(1, inner):
        src = (b + inner - o) % inner
        arrive(r_ab.at[src], sem_a.at[0, 1, src])
    for o in range(1, inner):
        src = (b + inner - o) % inner
        arrive(r_af.at[src], sem_a.at[1, 1, src])

    scale = [spread(jnp.exp(cta[a * inner + k, b])) for k in range(inner)]
    tot_f = r_af[0].astype(F32)
    for k in range(1, inner):
        tot_f = tot_f * scale[k] + r_af[k].astype(F32)
    tot_b = r_ab[inner - 1].astype(F32)
    for k in range(inner - 2, -1, -1):
        tot_b = tot_b * scale[k] + r_ab[k].astype(F32)
    s_bf[...] = tot_f.astype(BF16)
    s_bb[...] = tot_b.astype(BF16)
    for o in range(1, outer):
        up = (a + o) % outer
        down = (a + outer - o) % outer
        send(s_bf, r_bf.at[o], sem_b.at[0, 0, o], sem_b.at[0, 1, o], at_outer(up), a + o < outer)
        send(s_bb, r_bb.at[o], sem_b.at[1, 0, o], sem_b.at[1, 1, o], at_outer(down), a >= o)

    for g in range(cut1, cut2):
        within(g)

    acc_f[...] = jnp.zeros_like(acc_f)
    acc_b[...] = jnp.zeros_like(acc_b)
    wgt_f[...] = jnp.zeros_like(wgt_f)
    wgt_b[...] = jnp.zeros_like(wgt_b)
    for o in range(1, outer):

        @pl.when(a >= o)
        def _():
            arrive(r_bf.at[o], sem_b.at[0, 1, o])
            acc_f[...] += spread(jnp.exp(wgt_f[...])) * r_bf[o].astype(F32)
            for k in range(inner):
                wgt_f[...] += cta[(a - o) * inner + k, b]

        @pl.when(a + o < outer)
        def _():
            arrive(r_bb.at[o], sem_b.at[1, 1, o])
            acc_b[...] += spread(jnp.exp(wgt_b[...])) * r_bb[o].astype(F32)
            for k in range(inner):
                wgt_b[...] += cta[(a + o) * inner + k, b]

    run = acc_f[...]
    for k in range(inner):
        s_cf[k] = run.astype(BF16)
        if k < inner - 1:
            run = run * scale[k] + r_af[k].astype(F32)
    run = acc_b[...]
    for k in range(inner - 1, -1, -1):
        s_cb[k] = run.astype(BF16)
        if k > 0:
            run = run * scale[k] + r_ab[k].astype(F32)
    for o in range(1, inner):
        peer = (b + o) % inner
        send(s_cf.at[peer], r_cf.at[b], sem_c.at[0, 0, o], sem_c.at[0, 1, b], at_plane(peer))
        send(s_cb.at[peer], r_cb.at[b], sem_c.at[1, 0, o], sem_c.at[1, 1, b], at_plane(peer))
    r_cf[b] = s_cf[b]
    r_cb[b] = s_cb[b]

    for g in range(cut2, groups):
        within(g)

    for o in range(1, inner):
        src = (b + inner - o) % inner
        arrive(r_cf.at[src], sem_c.at[0, 1, src])
        arrive(r_cb.at[src], sem_c.at[1, 1, src])
    state = jnp.concatenate([r_cf[k] for k in range(inner)], axis=0)
    back = jnp.concatenate([r_cb[k] for k in range(inner)], axis=0)

    for g in range(groups):
        gs = slice(g * STATE, (g + 1) * STATE)
        cs = slice(g * gcols, (g + 1) * gcols)
        dk_s[:, gs] += dot(wu[:, cs], back[cs])
    cgrad = dk_s[...] * slope[...]
    ext[pl.ds(0, tokens)] = cgrad
    send(
        ext.at[pl.ds(0, 8)],
        halo,
        sem_halo.at[2],
        sem_halo.at[3],
        {"sp": (i + nsp - 1) % nsp},
        i > 0,
    )

    ones_row = jnp.ones((8, STATE), F32)
    for g in range(groups):
        gs = slice(g * STATE, (g + 1) * STATE)
        cs = slice(g * gcols, (g + 1) * gcols)
        dq_s[:, gs] += dot(edy[:, cs], state[cs])
        y_s[:, cs] += ece_s[:, cs] * dot(qry_ref[:, gs], state[cs], 1, 1)
    qg_ref[...] = dq_s[...].astype(BF16)

    @pl.when(i < nsp - 1)
    def _():
        arrive(halo, sem_halo.at[3])
        ext[pl.ds(tokens, 8)] = halo[...]

    @pl.when(i == nsp - 1)
    def _():
        ext[pl.ds(tokens, 8)] = jnp.zeros((8, chans), F32)

    pgrad = taps[0:1] * ext[pl.ds(ntap - 1, tokens)]
    for k in range(1, ntap):
        pgrad = pgrad + taps[k : k + 1] * ext[pl.ds(ntap - 1 - k, tokens)]
    pg = pgrad.astype(BF16)
    gbuf[a] = pg
    for o in range(1, outer):
        peer = (a + o) % outer
        send(gbuf.at[a], gbuf.at[a], sem_d.at[0, o], sem_d.at[1, a], at_outer(peer))

    for k in range(ntp):
        s_i[k] = dot(pg, w_ref[:, k * fchunk : (k + 1) * fchunk]).astype(BF16)
    for o in range(1, ntp):
        peer = (p + o) % ntp
        send(s_i.at[peer], r_i.at[p], sem_i.at[0, o], sem_i.at[1, p], {"tp": peer})
    r_i[p] = s_i[p]

    inter = []
    for g in range(groups):
        gs = slice(g * STATE, (g + 1) * STATE)
        cs = slice(g * gcols, (g + 1) * gcols)
        kg = wee_s[:, cs] * dot(keys[:, gs], back[cs], 1, 1)
        du_s[:, cs] += kg
        carry = dot(jnp.ones((8, tokens), F32), u_s[:, cs].astype(F32) * kg, precision=HIGHEST)
        both = state[cs].astype(F32) * back[cs].astype(F32)
        carry = carry + ece_s[tokens - 1 : tokens, cs] * dot(
            ones_row, both, 1, 1, precision=HIGHEST
        )
        inter.append(carry)
    inter = dot(jnp.concatenate(inter, axis=1), expand, 1, 1, precision=HIGHEST)[0:1]
    vg_ref[...] = (du_s[...] * dte_s[...]).astype(BF16)
    adj = adj_ref[...].astype(F32)
    gate2 = gate_ref[...].astype(F32)
    gg_ref[...] = (adj * y_s[...] * silu_slope(gate2)).astype(BF16)
    moved = dy_s[...].astype(F32) * y_s[...] - u_s[...].astype(F32) * du_s[...]
    dcum = dot(moved, expand, 1, 1, precision=HIGHEST)
    ddecay = dot(upper, dcum, precision=HIGHEST) + inter
    dstep = dot(val_ref[...].astype(F32) * du_s[...], expand, 1, 1, precision=HIGHEST)
    dg_ref[...] = (dstep - rate * ddecay) * jax.nn.sigmoid(pre)

    for o in range(1, outer):
        src = (a + outer - o) % outer
        arrive(xbuf.at[src], sem_x.at[1, src])
    grads = dot(gbuf[a], xbuf[a], 0, 0)
    for o in range(1, outer):
        src = (a + outer - o) % outer
        arrive(gbuf.at[src], sem_d.at[1, src])
        grads = grads + dot(gbuf[src], xbuf[src], 0, 0)
    for k in range(inner):
        part = grads[:, k * piece : (k + 1) * piece]
        rsum[k] = part
        s_r[k] = part.astype(BF16)
    for o in range(1, inner):
        peer = (b + o) % inner
        send(s_r.at[peer], r_r.at[b], sem_r.at[0, o], sem_r.at[1, b], at_plane(peer))

    for o in range(1, ntp):
        src = (p + ntp - o) % ntp
        arrive(r_i.at[src], sem_i.at[1, src])
    summed = r_i[0].astype(F32)
    for k in range(1, ntp):
        summed = summed + r_i[k].astype(F32)
    ig_ref[...] = summed.T.astype(BF16)

    kwg = rsum[b]
    for o in range(1, inner):
        src = (b + inner - o) % inner
        arrive(r_r.at[src], sem_r.at[1, src])
        kwg = kwg + r_r[src].astype(F32)
    squares = dot(jnp.ones((8, piece), F32), kwg * kwg, 1, 1, precision=HIGHEST)
    sq[i] = squares[0:1]
    for o in range(1, nsp):
        peer = (i + o) % nsp
        send(sq.at[i], sq.at[i], sem_q.at[0, o], sem_q.at[1, i], {"sp": peer})
    kwg_ref[...] = kwg
    for o in range(1, nsp):
        src = (i + nsp - o) % nsp
        arrive(sq.at[src], sem_q.at[1, src])
    result = sq[0]
    for k in range(1, nsp):
        result = result + sq[k]
    rows_ref[...] = result

    for copy, when in pending:
        if when is None:
            copy.wait_send()
        else:
            pl.when(when)(copy.wait_send)


def per_device(cfg, *args):
    x, w, taps, val, qry, pre, damp, jump, gate, adj = args
    nsp, ntp, outer, inner = cfg
    tokens, feats = x.shape
    chans = w.shape[0]
    heads = pre.shape[1]
    width = val.shape[1]
    qheads = heads // inner
    qrows = width // inner
    piece = feats // nsp
    fchunk = feats // ntp
    dma = pltpu.SemaphoreType.DMA
    V = pltpu.VMEM
    scratch = [
        V((16, feats), BF16),
        V((tokens + 16, chans), F32),
        V((tokens, chans), F32),
        V((nsp, inner, qheads, STATE), F32),
        V((tokens, width), BF16),
        V((tokens, width), BF16),
        V((tokens, width), F32),
        V((tokens, width), F32),
        V((tokens, width), F32),
        V((tokens, width), F32),
        V((tokens, width), F32),
        V((tokens, chans), F32),
        V((tokens, chans), F32),
        V((width, STATE), BF16),
        V((width, STATE), BF16),
        V((inner, qrows, STATE), BF16),
        V((inner, qrows, STATE), BF16),
        V((qrows, STATE), BF16),
        V((qrows, STATE), BF16),
        V((outer, qrows, STATE), BF16),
        V((outer, qrows, STATE), BF16),
        V((qrows, STATE), F32),
        V((qrows, STATE), F32),
        V((qheads, STATE), F32),
        V((qheads, STATE), F32),
        V((inner, qrows, STATE), BF16),
        V((inner, qrows, STATE), BF16),
        V((inner, qrows, STATE), BF16),
        V((inner, qrows, STATE), BF16),
        V((tokens + 8, chans), F32),
        V((8, chans), F32),
        V((outer, tokens, chans), BF16),
        V((outer, tokens, feats // outer), BF16),
        V((inner, chans, piece), F32),
        V((inner, chans, piece), BF16),
        V((inner, chans, piece), BF16),
        V((ntp, tokens, fchunk), BF16),
        V((ntp, tokens, fchunk), BF16),
        V((nsp, 1, chans), F32),
        dma((4,)),
        dma((2, nsp)),
        dma((2, 2, inner)),
        dma((2, 2, outer)),
        dma((2, 2, inner)),
        dma((2, outer)),
        dma((2, outer)),
        dma((2, inner)),
        dma((2, ntp)),
        dma((2, nsp)),
    ]
    out_shape = (
        jax.ShapeDtypeStruct((chans, piece), F32),
        jax.ShapeDtypeStruct((1, chans), F32),
        jax.ShapeDtypeStruct((fchunk, tokens), BF16),
        jax.ShapeDtypeStruct((tokens, width), BF16),
        jax.ShapeDtypeStruct((tokens, chans), BF16),
        jax.ShapeDtypeStruct((tokens, heads), F32),
        jax.ShapeDtypeStruct((tokens, width), BF16),
    )
    vmem = pl.BlockSpec(memory_space=pltpu.VMEM)
    outs = pl.pallas_call(
        functools.partial(kernel, cfg),
        out_shape=out_shape,
        in_specs=[vmem] * 10,
        out_specs=(vmem,) * 7,
        scratch_shapes=scratch,
        compiler_params=pltpu.CompilerParams(
            collective_id=0, has_side_effects=True, vmem_limit_bytes=56 * 2**20
        ),
    )(x, w, taps, val, qry, pre, damp.reshape(1, heads), jump, gate, adj)
    return (outs[0], outs[1].reshape(chans)) + tuple(outs[2:])


def solution(mesh):
    nsp, ntp = mesh.shape["sp"], mesh.shape["tp"]
    inner = 4
    cfg = (nsp, ntp, nsp // inner, inner)
    tokens = P("sp", "tp")
    in_specs = (
        P("sp", None),
        P("tp", None),
        P(None, "tp"),
        tokens,
        tokens,
        tokens,
        P("tp"),
        tokens,
        tokens,
        tokens,
    )
    out_specs = (P("tp", "sp"), P("tp"), P("tp", "sp"), tokens, tokens, tokens, tokens)
    return jax.shard_map(
        functools.partial(per_device, cfg),
        mesh=mesh,
        in_specs=in_specs,
        out_specs=out_specs,
        check_vma=False,
    )
```

time: 321 us -> 78.8 us (0.25)
  waiting for transfers between devices: 144 us -> 0 us
  Pallas kernels: 0 us -> 64.9 us
  blocking collectives: 40.5 us -> 0 us
  other arithmetic: 33.2 us -> 0 us
  matrix products: 32.9 us -> 0 us
  local copies, waits for them, and re-layouts: 35 us -> 12.9 us
  starting transfers between devices: 19.5 us -> 0 us
  between operations: 14.4 us -> 0.65 us
    ppermute x13 -> x0, waiting for transfers between devices: 89.7 us -> none  [the longest x11 85.5 us: from_partner(): return lax.ppermute(block, axis, route)]
    pallas_call x0 -> x1, Pallas kernels: none -> 64.9 us  [per_device(): pl.pallas_call(functools.partial(kernel, cfg), out_shape=out_shape, in_sp...]
    reduce_scatter x2 -> x0, waiting for transfers between devices: 53.8 us -> none  [the longest x1 53.7 us: per_device(): lax.psum_scatter(lax.dot_general(block_source, projected_grad, (((0,), (0...]
    psum x1 -> x0, blocking collectives: 40.5 us -> none  [per_device(): row_squares = lax.psum(jnp.sum(summed * summed, axis=0), 'sp')]
    dot_general x15 -> x0, matrix products: 32.9 us -> none  [the longest x3 11.5 us: block_step(): jnp.einsum('gij,ijgr,jgrp->igrp', scores, decay_mat, scaled, precision=HI...]
    ppermute x13 -> x0, starting transfers between devices: 19.3 us -> none  [the longest x11 15.5 us: from_partner(): return lax.ppermute(block, axis, route)]
    reduce_sum x4 -> x0, other arithmetic: 8.79 us -> none  [the longest x1 4 us: block_step(): carry_state * jnp.exp(end_decay)[..., None, None]]
    reshape x7 -> x0, local copies, waits for them, and re-layouts: 7.71 us -> none  [the longest x1 2.09 us: linear_scan_update(): return (outputs.reshape(tokens, -1), final_state)]
  transfers between devices with their start and end apart: 15 -> 0, of which waited for: 11 -> 0; matrix products, arithmetic and copies ran while one was open for 24% -> 0% of each run, Pallas kernels for 0% -> 0%
where the time goes in v1:
time: 78.8 us; the launch traced here: 78.4 us
  Pallas kernels  64.9 us (82%)
  local copies, waits for them, and re-layouts  12.9 us (16%)
    pallas_call x1, Pallas kernels, per_device(): pl.pallas_call(functools.partial(kernel, cfg), out_shape=out_shape, in_sp...  64.9 us
    unnamed x11, local copies, waits for them, and re-layouts  12.9 us

profile of v1, /device:TPU:0, one launch (start us, length us, event | category | flops | bytes accessed | tf_op | source)
XLA Modules:
  0.0 78.4 jit_solution(6010732902362330618)
XLA Ops:
  0.6 1.4 %copy.17.pre_ref = f32[128,16]{1,0:T(8,128)} copy(f32[128,16]{0,1:T(8,128)} %param.15) | data formatting | bytes 16384 | tf_op args[5]
  2.1 1.4 %copy.18.jump_ref = f32[128,16]{1,0:T(8,128)} copy(f32[128,16]{0,1:T(8,128)} %param.17) | data formatting | bytes 16384 | tf_op args[7]
  3.5 64.9 %shard_map.153 = (f32[512,128]{1,0:T(8,128)}, f32[1,512]{1,0:T(1,128)}, bf16[1024,128]{1,0:T(8,128)(2,1)}, bf16[128,1024]{1,0:T(8,128)(2,1)}, bf16[128,512]{1,0:...) custom-call(bf16[128,2048]{1,0:T(8,128)(2,1)} %x_ref.1, bf16[512,2048]{1,0:T(8,128)(2,1)} %w_ref.1, ...), custom_call_target="tpu_custom_call" | custom-call | tf_op jit(solution)/shard_map/pallas_call | solution.py:565
  68.3 0.0 copy-start
  68.4 1.6 %copy.19 = f32[128,16]{0,1:T(8,128)} copy(f32[128,16]{1,0:T(8,128)} %get-tuple-element.26) | data formatting | bytes 16384
  69.9 1.7 %copy.26 = f32[512,128]{1,0:T(8,128)} copy(f32[512,128]{1,0:T(8,128)} %get-tuple-element.35) | data formatting | bytes 524288
  71.6 1.3 %copy.27 = f32[512]{0:T(512)} copy(f32[512]{0:T(512)} %bitcast.2) | data formatting | bytes 4096
  72.8 1.7 %copy.28 = bf16[1024,128]{1,0:T(8,128)(2,1)} copy(bf16[1024,128]{1,0:T(8,128)(2,1)} %get-tuple-element.37) | data formatting | bytes 524288
  74.5 1.7 %copy.29 = bf16[128,1024]{1,0:T(8,128)(2,1)} copy(bf16[128,1024]{1,0:T(8,128)(2,1)} %get-tuple-element.38) | data formatting | bytes 524288
  76.2 1.6 %copy.30 = bf16[128,512]{1,0:T(8,128)(2,1)} copy(bf16[128,512]{1,0:T(8,128)(2,1)} %get-tuple-element.39) | data formatting | bytes 262144
  77.7 0.0 copy-done
  77.7 0.7 copy.31
Async XLA Ops:
  68.3 9.4 %copy-start = (bf16[128,1024]{1,0:T(8,128)(2,1)S(1)}, bf16[128,1024]{1,0:T(8,128)(2,1)}, u32[]{:S(2)}) copy-start(bf16[128,1024]{1,0:T(8,128)(2,1)} %get-tuple-element.41) | copy-start | bytes 786436

commit v2 on v1

--- a/solution.py
+++ b/solution.py
@@ -31,8 +31,8 @@
 
 def kernel(
     cfg,
-    x_ref,
-    w_ref,
+    x_hbm,
+    w_hbm,
     taps_ref,
     val_ref,
     qry_ref,
@@ -48,6 +48,8 @@
     qg_ref,
     dg_ref,
     gg_ref,
+    x_ref,
+    w_ref,
     xh,
     pext,
     slope,
@@ -97,6 +99,8 @@
     sem_r,
     sem_i,
     sem_q,
+    sem_y,
+    sem_l,
 ):
     nsp, ntp, outer, inner = cfg
     i = lax.axis_index("sp")
@@ -105,7 +109,7 @@
     b = i % inner
     tokens, feats = x_ref.shape
     chans = w_ref.shape[0]
-    heads = pre_ref.shape[1]
+    heads = pre_ref.shape[0]
     hdim = val_ref.shape[1] // heads
     groups = chans // STATE
     gcols = val_ref.shape[1] // groups
@@ -114,7 +118,14 @@
     span = feats // outer
     piece = feats // nsp
     fchunk = feats // ntp
-
+    share = tokens // ntp
+    halves = gbuf.shape[0]
+    hchan = chans // halves
+
+    load_x = pltpu.make_async_copy(x_hbm, x_ref, sem_l.at[0])
+    load_w = pltpu.make_async_copy(w_hbm, w_ref, sem_l.at[1])
+    load_x.start()
+    load_w.start()
     barrier = pltpu.get_barrier_semaphore()
     for o in range(1, nsp):
         pl.semaphore_signal(
@@ -159,30 +170,16 @@
     ec = lax.broadcasted_iota(jnp.int32, (heads, heads * hdim), 1)
     expand = (ec // hdim == eh).astype(F32)
 
-    pre = pre_ref[...]
+    pre = pre_ref[...].T
     rate = jnp.exp(damp_ref[...])
     step = jnp.maximum(pre, 0.0) + jnp.log1p(jnp.exp(-jnp.abs(pre)))
-    decay = jump_ref[...] - rate * step
+    decay = jump_ref[...].T - rate * step
     cum = dot(lower, decay, precision=HIGHEST)
     cum_t = dot(decay, upper, 0, 0, precision=HIGHEST)
     total = dot(decay, jnp.ones((tokens, STATE), F32), 0, 0, precision=HIGHEST)
     for k in range(inner):
         cta[i, k] = total[k * qheads : (k + 1) * qheads]
     end = cum[tokens - 1 : tokens]
-
-    pl.semaphore_wait(barrier, nsp - 1 + ntp - 1)
-
-    send(
-        x_ref.at[pl.ds(tokens - 16, 16)],
-        xh,
-        sem_halo.at[0],
-        sem_halo.at[1],
-        {"sp": (i + 1) % nsp},
-        i < nsp - 1,
-    )
-    for o in range(1, nsp):
-        peer = (i + o) % nsp
-        send(cta.at[i], cta.at[i], sem_ct.at[0, o], sem_ct.at[1, i], {"sp": peer})
 
     ece = dot(jnp.exp(cum), expand, precision=HIGHEST)
     ece_s[...] = ece
@@ -194,8 +191,14 @@
         cs = slice(g * gcols, (g + 1) * gcols)
         part = dot(edy[:, cs], qry_ref[:, g * STATE : (g + 1) * STATE], 0, 0)
         s_ab[pl.ds(g * gcols, gcols)] = part.astype(BF16)
+    load_x.wait()
+
+    pl.semaphore_wait(barrier, nsp - 1 + ntp - 1)
+
     for o in range(1, inner):
         peer = (b + o) % inner
+        other = a * inner + peer
+        send(cta.at[i], cta.at[i], sem_ct.at[0, other], sem_ct.at[1, i], {"sp": other})
         send(
             s_ab.at[pl.ds(pl.multiple_of(peer * qrows, qrows), qrows)],
             r_ab.at[b],
@@ -203,13 +206,26 @@
             sem_a.at[0, 1, b],
             at_plane(peer),
         )
+    send(
+        x_ref.at[pl.ds(tokens - 16, 16)],
+        xh,
+        sem_halo.at[0],
+        sem_halo.at[1],
+        {"sp": (i + 1) % nsp},
+        i < nsp - 1,
+    )
+    for o in range(1, outer):
+        for k in range(inner):
+            other = (a + o) % outer * inner + k
+            send(cta.at[i], cta.at[i], sem_ct.at[0, other], sem_ct.at[1, i], {"sp": other})
     r_ab[b] = s_ab[pl.ds(pl.multiple_of(b * qrows, qrows), qrows)]
 
+    mine = pl.ds(pl.multiple_of(p * share, share), share)
     for o in range(1, outer):
         peer = (a + o) % outer
         send(
-            x_ref.at[:, pl.ds(pl.multiple_of(peer * span, span), span)],
-            xbuf.at[a],
+            x_ref.at[mine, pl.ds(pl.multiple_of(peer * span, span), span)],
+            xbuf.at[a, mine],
             sem_x.at[0, o],
             sem_x.at[1, a],
             at_outer(peer),
@@ -224,6 +240,7 @@
     u_s[...] = scaled.astype(BF16)
     wu = (scaled * wee).astype(BF16)
 
+    load_w.wait()
     proj = dot(x_ref[...], w_ref[...], 1, 1)
     pext[pl.ds(16, tokens)] = proj.astype(BF16).astype(F32)
 
@@ -281,15 +298,6 @@
         dq_s[:, gs] = dot(ds, key)
         dk_s[:, gs] = dot(ds, q, 0, 0)
 
-    cut1 = (groups + 1) // 2
-    cut2 = cut1 + (groups - cut1 + 1) // 2
-    for g in range(cut1):
-        within(g)
-
-    for o in range(1, nsp):
-        src = (i + nsp - o) % nsp
-        arrive(cta.at[src], sem_ct.at[1, src])
-
     def spread(rows):
         return jnp.concatenate(
             [jnp.broadcast_to(rows[h : h + 1], (hdim, STATE)) for h in range(qheads)], axis=0
@@ -297,33 +305,76 @@
 
     for o in range(1, inner):
         src = (b + inner - o) % inner
+        arrive(cta.at[a * inner + src], sem_ct.at[1, a * inner + src])
         arrive(r_ab.at[src], sem_a.at[0, 1, src])
+    scale = [spread(jnp.exp(cta[a * inner + k, b])) for k in range(inner)]
+    tot_b = r_ab[inner - 1].astype(F32)
+    for k in range(inner - 2, -1, -1):
+        tot_b = tot_b * scale[k] + r_ab[k].astype(F32)
+    s_bb[...] = tot_b.astype(BF16)
+    for o in range(1, outer):
+        down = (a + outer - o) % outer
+        send(s_bb, r_bb.at[o], sem_b.at[1, 0, o], sem_b.at[1, 1, o], at_outer(down), a >= o)
+
+    cut = (groups + 1) // 2
+    within(0)
+
     for o in range(1, inner):
         src = (b + inner - o) % inner
         arrive(r_af.at[src], sem_a.at[1, 1, src])
-
-    scale = [spread(jnp.exp(cta[a * inner + k, b])) for k in range(inner)]
     tot_f = r_af[0].astype(F32)
     for k in range(1, inner):
         tot_f = tot_f * scale[k] + r_af[k].astype(F32)
-    tot_b = r_ab[inner - 1].astype(F32)
-    for k in range(inner - 2, -1, -1):
-        tot_b = tot_b * scale[k] + r_ab[k].astype(F32)
     s_bf[...] = tot_f.astype(BF16)
-    s_bb[...] = tot_b.astype(BF16)
     for o in range(1, outer):
         up = (a + o) % outer
-        down = (a + outer - o) % outer
         send(s_bf, r_bf.at[o], sem_b.at[0, 0, o], sem_b.at[0, 1, o], at_outer(up), a + o < outer)
-        send(s_bb, r_bb.at[o], sem_b.at[1, 0, o], sem_b.at[1, 1, o], at_outer(down), a >= o)
-
-    for g in range(cut1, cut2):
+
+    for o in range(1, outer):
+        src = (a + outer - o) % outer
+        arrive(xbuf.at[src, mine], sem_x.at[1, src])
+        for t in range(1, ntp):
+            send(
+                xbuf.at[src, mine],
+                xbuf.at[src, mine],
+                sem_y.at[0, o, t],
+                sem_y.at[1, src, p],
+                {"tp": (p + t) % ntp},
+            )
+
+    for g in range(1, cut):
         within(g)
+    for o in range(1, outer):
+        for k in range(inner):
+            src = (a + outer - o) % outer * inner + k
+            arrive(cta.at[src], sem_ct.at[1, src])
+
+    acc_b[...] = jnp.zeros_like(acc_b)
+    wgt_b[...] = jnp.zeros_like(wgt_b)
+    for o in range(1, outer):
+
+        @pl.when(a + o < outer)
+        def _():
+            arrive(r_bb.at[o], sem_b.at[1, 1, o])
+            acc_b[...] += spread(jnp.exp(wgt_b[...])) * r_bb[o].astype(F32)
+            for k in range(inner):
+                wgt_b[...] += cta[(a + o) * inner + k, b]
+
+    run = acc_b[...]
+    for k in range(inner - 1, -1, -1):
+        s_cb[k] = run.astype(BF16)
+        if k > 0:
+            run = run * scale[k] + r_ab[k].astype(F32)
+    for o in range(1, inner):
+        peer = (b + o) % inner
+        send(s_cb.at[peer], r_cb.at[b], sem_c.at[1, 0, o], sem_c.at[1, 1, b], at_plane(peer))
+    r_cb[b] = s_cb[b]
+
+    for g in range(cut, groups):
+        within(g)
 
     acc_f[...] = jnp.zeros_like(acc_f)
-    acc_b[...] = jnp.zeros_like(acc_b)
     wgt_f[...] = jnp.zeros_like(wgt_f)
-    wgt_b[...] = jnp.zeros_like(wgt_b)
     for o in range(1, outer):
 
         @pl.when(a >= o)
@@ -333,38 +384,19 @@
             for k in range(inner):
                 wgt_f[...] += cta[(a - o) * inner + k, b]
 
-        @pl.when(a + o < outer)
-        def _():
-            arrive(r_bb.at[o], sem_b.at[1, 1, o])
-            acc_b[...] += spread(jnp.exp(wgt_b[...])) * r_bb[o].astype(F32)
-            for k in range(inner):
-                wgt_b[...] += cta[(a + o) * inner + k, b]
-
     run = acc_f[...]
     for k in range(inner):
         s_cf[k] = run.astype(BF16)
         if k < inner - 1:
             run = run * scale[k] + r_af[k].astype(F32)
-    run = acc_b[...]
-    for k in range(inner - 1, -1, -1):
-        s_cb[k] = run.astype(BF16)
-        if k > 0:
-            run = run * scale[k] + r_ab[k].astype(F32)
     for o in range(1, inner):
         peer = (b + o) % inner
         send(s_cf.at[peer], r_cf.at[b], sem_c.at[0, 0, o], sem_c.at[0, 1, b], at_plane(peer))
-        send(s_cb.at[peer], r_cb.at[b], sem_c.at[1, 0, o], sem_c.at[1, 1, b], at_plane(peer))
     r_cf[b] = s_cf[b]
-    r_cb[b] = s_cb[b]
-
-    for g in range(cut2, groups):
-        within(g)
 
     for o in range(1, inner):
         src = (b + inner - o) % inner
-        arrive(r_cf.at[src], sem_c.at[0, 1, src])
         arrive(r_cb.at[src], sem_c.at[1, 1, src])
-    state = jnp.concatenate([r_cf[k] for k in range(inner)], axis=0)
     back = jnp.concatenate([r_cb[k] for k in range(inner)], axis=0)
 
     for g in range(groups):
@@ -382,7 +414,54 @@
         i > 0,
     )
 
-    ones_row = jnp.ones((8, STATE), F32)
+    def backs(g):
+        gs = slice(g * STATE, (g + 1) * STATE)
+        cs = slice(g * gcols, (g + 1) * gcols)
+        return wee_s[:, cs] * dot(keys[:, gs], back[cs], 1, 1)
+
+    pulled = [backs(g) for g in range(groups)]
+    for g in range(groups):
+        cs = slice(g * gcols, (g + 1) * gcols)
+        du_s[:, cs] += pulled[g]
+    vg_ref[...] = (du_s[...] * dte_s[...]).astype(BF16)
+
+    @pl.when(i < nsp - 1)
+    def _():
+        arrive(halo, sem_halo.at[3])
+        ext[pl.ds(tokens, 8)] = halo[...]
+
+    @pl.when(i == nsp - 1)
+    def _():
+        ext[pl.ds(tokens, 8)] = jnp.zeros((8, chans), F32)
+
+    pgrad = taps[0:1] * ext[pl.ds(ntap - 1, tokens)]
+    for k in range(1, ntap):
+        pgrad = pgrad + taps[k : k + 1] * ext[pl.ds(ntap - 1 - k, tokens)]
+    pg = pgrad.astype(BF16)
+    for f in range(halves):
+        gbuf[f, a] = pg[:, f * hchan : (f + 1) * hchan]
+    for f in range(halves):
+        for o in range(1, outer):
+            peer = (a + o) % outer
+            send(
+                gbuf.at[f, a],
+                gbuf.at[f, a],
+                sem_d.at[0, f, o],
+                sem_d.at[1, f, a],
+                at_outer(peer),
+            )
+
+    for k in range(ntp):
+        s_i[k] = dot(pg, w_ref[:, k * fchunk : (k + 1) * fchunk]).astype(BF16)
+    for o in range(1, ntp):
+        peer = (p + o) % ntp
+        send(s_i.at[peer], r_i.at[p], sem_i.at[0, o], sem_i.at[1, p], {"tp": peer})
+    r_i[p] = s_i[p]
+
+    for o in range(1, inner):
+        src = (b + inner - o) % inner
+        arrive(r_cf.at[src], sem_c.at[0, 1, src])
+    state = jnp.concatenate([r_cf[k] for k in range(inner)], axis=0)
     for g in range(groups):
         gs = slice(g * STATE, (g + 1) * STATE)
         cs = slice(g * gcols, (g + 1) * gcols)
@@ -390,69 +469,31 @@
         y_s[:, cs] += ece_s[:, cs] * dot(qry_ref[:, gs], state[cs], 1, 1)
     qg_ref[...] = dq_s[...].astype(BF16)
 
-    @pl.when(i < nsp - 1)
-    def _():
-        arrive(halo, sem_halo.at[3])
-        ext[pl.ds(tokens, 8)] = halo[...]
-
-    @pl.when(i == nsp - 1)
-    def _():
-        ext[pl.ds(tokens, 8)] = jnp.zeros((8, chans), F32)
-
-    pgrad = taps[0:1] * ext[pl.ds(ntap - 1, tokens)]
-    for k in range(1, ntap):
-        pgrad = pgrad + taps[k : k + 1] * ext[pl.ds(ntap - 1 - k, tokens)]
-    pg = pgrad.astype(BF16)
-    gbuf[a] = pg
-    for o in range(1, outer):
-        peer = (a + o) % outer
-        send(gbuf.at[a], gbuf.at[a], sem_d.at[0, o], sem_d.at[1, a], at_outer(peer))
-
-    for k in range(ntp):
-        s_i[k] = dot(pg, w_ref[:, k * fchunk : (k + 1) * fchunk]).astype(BF16)
-    for o in range(1, ntp):
-        peer = (p + o) % ntp
-        send(s_i.at[peer], r_i.at[p], sem_i.at[0, o], sem_i.at[1, p], {"tp": peer})
-    r_i[p] = s_i[p]
-
-    inter = []
-    for g in range(groups):
-        gs = slice(g * STATE, (g + 1) * STATE)
-        cs = slice(g * gcols, (g + 1) * gcols)
-        kg = wee_s[:, cs] * dot(keys[:, gs], back[cs], 1, 1)
-        du_s[:, cs] += kg
-        carry = dot(jnp.ones((8, tokens), F32), u_s[:, cs].astype(F32) * kg, precision=HIGHEST)
-        both = state[cs].astype(F32) * back[cs].astype(F32)
-        carry = carry + ece_s[tokens - 1 : tokens, cs] * dot(
-            ones_row, both, 1, 1, precision=HIGHEST
-        )
-        inter.append(carry)
-    inter = dot(jnp.concatenate(inter, axis=1), expand, 1, 1, precision=HIGHEST)[0:1]
-    vg_ref[...] = (du_s[...] * dte_s[...]).astype(BF16)
-    adj = adj_ref[...].astype(F32)
-    gate2 = gate_ref[...].astype(F32)
-    gg_ref[...] = (adj * y_s[...] * silu_slope(gate2)).astype(BF16)
-    moved = dy_s[...].astype(F32) * y_s[...] - u_s[...].astype(F32) * du_s[...]
-    dcum = dot(moved, expand, 1, 1, precision=HIGHEST)
-    ddecay = dot(upper, dcum, precision=HIGHEST) + inter
-    dstep = dot(val_ref[...].astype(F32) * du_s[...], expand, 1, 1, precision=HIGHEST)
-    dg_ref[...] = (dstep - rate * ddecay) * jax.nn.sigmoid(pre)
-
     for o in range(1, outer):
         src = (a + outer - o) % outer
-        arrive(xbuf.at[src], sem_x.at[1, src])
-    grads = dot(gbuf[a], xbuf[a], 0, 0)
-    for o in range(1, outer):
-        src = (a + outer - o) % outer
-        arrive(gbuf.at[src], sem_d.at[1, src])
-        grads = grads + dot(gbuf[src], xbuf[src], 0, 0)
-    for k in range(inner):
-        part = grads[:, k * piece : (k + 1) * piece]
-        rsum[k] = part
-        s_r[k] = part.astype(BF16)
-    for o in range(1, inner):
-        peer = (b + o) % inner
-        send(s_r.at[peer], r_r.at[b], sem_r.at[0, o], sem_r.at[1, b], at_plane(peer))
+        for t in range(1, ntp):
+            q = (p + ntp - t) % ntp
+            rows = pl.ds(pl.multiple_of(q * share, share), share)
+            arrive(xbuf.at[src, rows], sem_y.at[1, src, q])
+    for f in range(halves):
+        grads = dot(gbuf[f, a], xbuf[a], 0, 0)
+        for o in range(1, outer):
+            src = (a + outer - o) % outer
+            arrive(gbuf.at[f, src], sem_d.at[1, f, src])
+            grads = grads + dot(gbuf[f, src], xbuf[src], 0, 0)
+        for k in range(inner):
+            part = grads[:, k * piece : (k + 1) * piece]
+            rsum[f, k] = part
+            s_r[f, k] = part.astype(BF16)
+        for o in range(1, inner):
+            peer = (b + o) % inner
+            send(
+                s_r.at[f, peer],
+                r_r.at[f, b],
+                sem_r.at[0, f, o],
+                sem_r.at[1, f, b],
+                at_plane(peer),
+            )
 
     for o in range(1, ntp):
         src = (p + ntp - o) % ntp
@@ -462,17 +503,41 @@
         summed = summed + r_i[k].astype(F32)
     ig_ref[...] = summed.T.astype(BF16)
 
-    kwg = rsum[b]
-    for o in range(1, inner):
-        src = (b + inner - o) % inner
-        arrive(r_r.at[src], sem_r.at[1, src])
-        kwg = kwg + r_r[src].astype(F32)
-    squares = dot(jnp.ones((8, piece), F32), kwg * kwg, 1, 1, precision=HIGHEST)
-    sq[i] = squares[0:1]
+    gg_ref[...] = (
+        adj_ref[...].astype(F32) * y_s[...] * silu_slope(gate_ref[...].astype(F32))
+    ).astype(BF16)
+
+    for f in range(halves):
+        kwg = rsum[f, b]
+        for o in range(1, inner):
+            src = (b + inner - o) % inner
+            arrive(r_r.at[f, src], sem_r.at[1, f, src])
+            kwg = kwg + r_r[f, src].astype(F32)
+        squares = dot(jnp.ones((8, piece), F32), kwg * kwg, 1, 1, precision=HIGHEST)
+        sq[i, :, f * hchan : (f + 1) * hchan] = squares[0:1]
+        kwg_ref[f * hchan : (f + 1) * hchan] = kwg
     for o in range(1, nsp):
         peer = (i + o) % nsp
         send(sq.at[i], sq.at[i], sem_q.at[0, o], sem_q.at[1, i], {"sp": peer})
-    kwg_ref[...] = kwg
+
+    inter = []
+    for g in range(groups):
+        cs = slice(g * gcols, (g + 1) * gcols)
+        carry = dot(
+            jnp.ones((8, tokens), F32), u_s[:, cs].astype(F32) * pulled[g], precision=HIGHEST
+        )
+        both = state[cs].astype(F32) * back[cs].astype(F32)
+        carry = carry + ece_s[tokens - 1 : tokens, cs] * dot(
+            jnp.ones((8, STATE), F32), both, 1, 1, precision=HIGHEST
+        )
+        inter.append(carry)
+    inter = dot(jnp.concatenate(inter, axis=1), expand, 1, 1, precision=HIGHEST)[0:1]
+    moved = dy_s[...].astype(F32) * y_s[...] - u_s[...].astype(F32) * du_s[...]
+    dcum = dot(moved, expand, 1, 1, precision=HIGHEST)
+    ddecay = dot(upper, dcum, precision=HIGHEST) + inter
+    dstep = dot(val_ref[...].astype(F32) * du_s[...], expand, 1, 1, precision=HIGHEST)
+    dg_ref[...] = ((dstep - rate * ddecay) * jax.nn.sigmoid(pre)).T
+
     for o in range(1, nsp):
         src = (i + nsp - o) % nsp
         arrive(sq.at[src], sem_q.at[1, src])
@@ -488,12 +553,19 @@
             pl.when(when)(copy.wait_send)
 
 
+def finish(*refs):
+    count = len(refs) // 2
+    for src, dst in zip(refs[:count], refs[count:]):
+        dst[...] = src[...]
+
+
 def per_device(cfg, *args):
     x, w, taps, val, qry, pre, damp, jump, gate, adj = args
     nsp, ntp, outer, inner = cfg
     tokens, feats = x.shape
     chans = w.shape[0]
     heads = pre.shape[1]
+    halves = 2 if chans > STATE else 1
     width = val.shape[1]
     qheads = heads // inner
     qrows = width // inner
@@ -502,6 +574,8 @@
     dma = pltpu.SemaphoreType.DMA
     V = pltpu.VMEM
     scratch = [
+        V((tokens, feats), BF16),
+        V((chans, feats), BF16),
         V((16, feats), BF16),
         V((tokens + 16, chans), F32),
         V((tokens, chans), F32),
@@ -533,11 +607,11 @@
         V((inner, qrows, STATE), BF16),
         V((tokens + 8, chans), F32),
         V((8, chans), F32),
-        V((outer, tokens, chans), BF16),
+        V((halves, outer, tokens, chans // halves), BF16),
         V((outer, tokens, feats // outer), BF16),
-        V((inner, chans, piece), F32),
-        V((inner, chans, piece), BF16),
-        V((inner, chans, piece), BF16),
+        V((halves, inner, chans // halves, piece), F32),
+        V((halves, inner, chans // halves, piece), BF16),
+        V((halves, inner, chans // halves, piece), BF16),
         V((ntp, tokens, fchunk), BF16),
         V((ntp, tokens, fchunk), BF16),
         V((nsp, 1, chans), F32),
@@ -547,10 +621,12 @@
         dma((2, 2, outer)),
         dma((2, 2, inner)),
         dma((2, outer)),
-        dma((2, outer)),
-        dma((2, inner)),
+        dma((2, halves, outer)),
+        dma((2, halves, inner)),
         dma((2, ntp)),
         dma((2, nsp)),
+        dma((2, outer, ntp)),
+        dma((2,)),
     ]
     out_shape = (
         jax.ShapeDtypeStruct((chans, piece), F32),
@@ -558,21 +634,28 @@
         jax.ShapeDtypeStruct((fchunk, tokens), BF16),
         jax.ShapeDtypeStruct((tokens, width), BF16),
         jax.ShapeDtypeStruct((tokens, chans), BF16),
-        jax.ShapeDtypeStruct((tokens, heads), F32),
+        jax.ShapeDtypeStruct((heads, tokens), F32),
         jax.ShapeDtypeStruct((tokens, width), BF16),
     )
     vmem = pl.BlockSpec(memory_space=pltpu.VMEM)
     outs = pl.pallas_call(
         functools.partial(kernel, cfg),
         out_shape=out_shape,
-        in_specs=[vmem] * 10,
+        in_specs=[pl.BlockSpec(memory_space=pl.ANY)] * 2 + [vmem] * 8,
         out_specs=(vmem,) * 7,
         scratch_shapes=scratch,
         compiler_params=pltpu.CompilerParams(
-            collective_id=0, has_side_effects=True, vmem_limit_bytes=56 * 2**20
+            collective_id=0, has_side_effects=True, vmem_limit_bytes=24 * 2**20
         ),
-    )(x, w, taps, val, qry, pre, damp.reshape(1, heads), jump, gate, adj)
-    return (outs[0], outs[1].reshape(chans)) + tuple(outs[2:])
+    )(x, w, taps, val, qry, pre.T, damp.reshape(1, heads), jump.T, gate, adj)
+    outs = pl.pallas_call(
+        finish,
+        out_shape=out_shape,
+        in_specs=[vmem] * 7,
+        out_specs=(vmem,) * 7,
+        compiler_params=pltpu.CompilerParams(vmem_limit_bytes=16 * 2**20),
+    )(*outs)
+    return (outs[0], outs[1].reshape(chans)) + tuple(outs[2:5]) + (outs[5].T, outs[6])
 
 
 def solution(mesh):

time: 78.8 us -> 63.4 us (0.80)
  Pallas kernels: 64.9 us -> 53.2 us
  local copies, waits for them, and re-layouts: 12.9 us -> 9.12 us
    pallas_call x1, Pallas kernels: 64.9 us -> 52.1 us  [per_device(): pl.pallas_call(functools.partial(kernel, cfg), out_shape=out_shape, in_sp...]
    unnamed x11 -> x20, local copies, waits for them, and re-layouts: 12.9 us -> 9.12 us
    pallas_call x0 -> x1, Pallas kernels: none -> 1.09 us  [per_device(): pl.pallas_call(finish, out_shape=out_shape, in_specs=[vmem] * 7, out_spec...]
where the time goes in v2:
time: 63.4 us; the launch traced here: 63 us
  Pallas kernels  53.2 us (84%)
  local copies, waits for them, and re-layouts  9.12 us (14%)
  between operations  0.66 us (1%)
    pallas_call x1, Pallas kernels, per_device(): pl.pallas_call(functools.partial(kernel, cfg), out_shape=out_shape, in_sp...  52.1 us
    unnamed x20, local copies, waits for them, and re-layouts  9.12 us

profile of v2, /device:TPU:0, one launch (start us, length us, event | category | flops | bytes accessed | tf_op | source)
XLA Modules:
  0.0 63.0 jit_solution(6204784581458055400)
XLA Ops:
  0.6 0.0 copy-start
  0.6 1.6 %copy-done = bf16[512,2048]{1,0:T(8,128)(2,1)S(1)} copy-done((bf16[512,2048]{1,0:T(8,128)(2,1)S(1)}, bf16[512,2048]{1,0:T(8,128)(2,1)}, u32[]{:S(2)}) %copy-start) | copy-done | bytes 2097176
  2.2 0.0 copy-start.1
  2.2 1.0 %copy-done.1 = bf16[128,2048]{1,0:T(8,128)(2,1)S(1)} copy-done((bf16[128,2048]{1,0:T(8,128)(2,1)S(1)}, bf16[128,2048]{1,0:T(8,128)(2,1)}, u32[]{:S(2)}) %copy-start.1) | copy-done | bytes 524312
  3.3 0.0 copy-start.2
  3.3 0.9 %copy-done.2 = bf16[128,1024]{1,0:T(8,128)(2,1)S(1)} copy-done((bf16[128,1024]{1,0:T(8,128)(2,1)S(1)}, bf16[128,1024]{1,0:T(8,128)(2,1)}, u32[]{:S(2)}) %copy-start.2) | copy-done | bytes 262168
  4.2 0.0 copy-start.3
  4.2 0.9 %copy-done.3 = bf16[128,1024]{1,0:T(8,128)(2,1)S(1)} copy-done((bf16[128,1024]{1,0:T(8,128)(2,1)S(1)}, bf16[128,1024]{1,0:T(8,128)(2,1)}, u32[]{:S(2)}) %copy-start.3) | copy-done | bytes 262168
  5.2 0.0 copy-start.4
  5.2 0.9 %copy-done.4 = bf16[128,1024]{1,0:T(8,128)(2,1)S(1)} copy-done((bf16[128,1024]{1,0:T(8,128)(2,1)S(1)}, bf16[128,1024]{1,0:T(8,128)(2,1)}, u32[]{:S(2)}) %copy-start.4) | copy-done | bytes 262168
  6.1 0.0 copy-start.5
  6.1 0.9 %copy-done.5 = bf16[128,512]{1,0:T(8,128)(2,1)S(1)} copy-done((bf16[128,512]{1,0:T(8,128)(2,1)S(1)}, bf16[128,512]{1,0:T(8,128)(2,1)}, u32[]{:S(2)}) %copy-start.5) | copy-done | bytes 131096
  7.0 0.0 copy-start.6
  7.0 0.7 %copy-done.6 = f32[4,512]{1,0:T(4,128)S(1)} copy-done((f32[4,512]{1,0:T(4,128)S(1)}, f32[4,512]{1,0:T(4,128)}, u32[]{:S(2)}) %copy-start.6) | copy-done | bytes 8216
  7.7 0.0 copy-start.7
  7.7 0.7 %copy-done.7 = f32[128,16]{0,1:T(8,128)S(1)} copy-done((f32[128,16]{0,1:T(8,128)S(1)}, f32[128,16]{0,1:T(8,128)}, u32[]{:S(2)}) %copy-start.7) | copy-done | bytes 8216
  8.4 0.0 copy-start.8
  8.4 0.7 %copy-done.8 = f32[128,16]{0,1:T(8,128)S(1)} copy-done((f32[128,16]{0,1:T(8,128)S(1)}, f32[128,16]{0,1:T(8,128)}, u32[]{:S(2)}) %copy-start.8) | copy-done | bytes 8216
  9.1 0.0 copy-start.9
  9.1 0.7 %copy-done.9 = f32[16]{0:T(128)S(1)} copy-done((f32[16]{0:T(128)S(1)}, f32[16]{0:T(128)}, u32[]{:S(2)}) %copy-start.9) | copy-done | bytes 88
  9.8 52.1 %shard_map.153 = (f32[512,128]{1,0:T(8,128)S(1)}, f32[1,512]{1,0:T(1,128)S(1)}, bf16[1024,128]{1,0:T(8,128)(2,1)S(1)}, bf16[128,1024]{1,0:T(8,128)(2,1)S(1)}, bf...) custom-call(bf16[128,2048]{1,0:T(8,128)(2,1)S(1)} %copy-done.1, ...), custom_call_target="tpu_custom_call" | custom-call | tf_op jit(solution)/shard_map/pallas_call | solution.py:641
  61.9 1.1 %shard_map.154 = (f32[512,128]{1,0:T(8,128)}, f32[1,512]{1,0:T(1,128)}, bf16[1024,128]{1,0:T(8,128)(2,1)}, bf16[128,1024]{1,0:T(8,128)(2,1)}, bf16[128,512]{1,0:...) custom-call(f32[512,128]{1,0:T(8,128)S(1)} %get-tuple-element.21.refs_0_, ...), custom_call_target="tpu_custom_call" | custom-call | tf_op jit(solution)/shard_map/pallas_call | solution.py:651
Async XLA Ops:
  0.6 1.6 %copy-start = (bf16[512,2048]{1,0:T(8,128)(2,1)S(1)}, bf16[512,2048]{1,0:T(8,128)(2,1)}, u32[]{:S(2)}) copy-start(bf16[512,2048]{1,0:T(8,128)(2,1)} %w_hbm.1) | copy-start | bytes 6291460
  2.2 1.0 %copy-start.1 = (bf16[128,2048]{1,0:T(8,128)(2,1)S(1)}, bf16[128,2048]{1,0:T(8,128)(2,1)}, u32[]{:S(2)}) copy-start(bf16[128,2048]{1,0:T(8,128)(2,1)} %x_hbm.1) | copy-start | bytes 1572868
  3.3 0.9 %copy-start.2 = (bf16[128,1024]{1,0:T(8,128)(2,1)S(1)}, bf16[128,1024]{1,0:T(8,128)(2,1)}, u32[]{:S(2)}) copy-start(bf16[128,1024]{1,0:T(8,128)(2,1)} %val_ref.1) | copy-start | bytes 786436
  4.2 0.9 %copy-start.3 = (bf16[128,1024]{1,0:T(8,128)(2,1)S(1)}, bf16[128,1024]{1,0:T(8,128)(2,1)}, u32[]{:S(2)}) copy-start(bf16[128,1024]{1,0:T(8,128)(2,1)} %gate_ref.1) | copy-start | bytes 786436
  5.2 0.9 %copy-start.4 = (bf16[128,1024]{1,0:T(8,128)(2,1)S(1)}, bf16[128,1024]{1,0:T(8,128)(2,1)}, u32[]{:S(2)}) copy-start(bf16[128,1024]{1,0:T(8,128)(2,1)} %adj_ref.1) | copy-start | bytes 786436
  6.1 0.9 %copy-start.5 = (bf16[128,512]{1,0:T(8,128)(2,1)S(1)}, bf16[128,512]{1,0:T(8,128)(2,1)}, u32[]{:S(2)}) copy-start(bf16[128,512]{1,0:T(8,128)(2,1)} %qry_ref.1) | copy-start | bytes 393220
  7.0 0.7 %copy-start.6 = (f32[4,512]{1,0:T(4,128)S(1)}, f32[4,512]{1,0:T(4,128)}, u32[]{:S(2)}) copy-start(f32[4,512]{1,0:T(4,128)} %taps_ref.1) | copy-start | bytes 24580
  7.7 0.7 %copy-start.7 = (f32[128,16]{0,1:T(8,128)S(1)}, f32[128,16]{0,1:T(8,128)}, u32[]{:S(2)}) copy-start(f32[128,16]{0,1:T(8,128)} %param.15) | copy-start | bytes 24580
  8.4 0.7 %copy-start.8 = (f32[128,16]{0,1:T(8,128)S(1)}, f32[128,16]{0,1:T(8,128)}, u32[]{:S(2)}) copy-start(f32[128,16]{0,1:T(8,128)} %param.17) | copy-start | bytes 24580
  9.1 0.7 %copy-start.9 = (f32[16]{0:T(128)S(1)}, f32[16]{0:T(128)}, u32[]{:S(2)}) copy-start(f32[16]{0:T(128)} %param.16) | copy-start | bytes 196
